TPU v7x, 256 devices: a whole 4x4x8 slice. The times are simulated.
256 devices in a mesh: fs: 32 (over z, x), tp: 8 (over y, core).
Axes of the slice: x: 4, y: 4, z: 8, core: 2. Of those that a mesh axis runs over, the one named last changes fastest.
Arguments:
- tokens: bfloat16 [32768, 2048], P('fs', 'tp'), may hold values from -6 to 6
- grad_out: bfloat16 [32768, 2048], P('fs', 'tp'), may hold values from -6 to 6
- norm_gain: float32 [2048], replicated, may hold values from 0.1 to 1.9
- gate_weight: bfloat16 [3072, 2048], P('tp', 'fs'), may hold values from -0.125 to 0.125
- up_weight: bfloat16 [3072, 2048], P('tp', 'fs'), may hold values from -0.125 to 0.125
- down_weight: bfloat16 [3072, 2048], P('tp', 'fs'), may hold values from -0.109375 to 0.109375
Outputs:
- grad_input: bfloat16 [32768, 2048], P('fs', 'tp')
- grad_gate: float32 [3072, 2048], P('tp', 'fs')
- grad_up: float32 [3072, 2048], P('tp', 'fs')
- grad_down: float32 [3072, 2048], P('tp', 'fs')
- row_squares: float32 [3, 3072], P(None, 'tp')
All inputs are finite; a program needn't handle non-finite values.
Results may differ from a plain program's by a relative error of at most 0.015.
Values may be sent and summed in bfloat16 or wider, within the bound.
A program may use at most 64 MiB of HBM per device.

v0:
```python
import jax
import jax.numpy as jnp
from jax import lax
from jax.sharding import Mesh
from jax.sharding import PartitionSpec as P

FS = ("fs_0", "fs_1")


def sent_together(arrays, axis, dim, along):
    widths = [a.shape[along] for a in arrays]
    both = jnp.concatenate(arrays, axis=along)
    whole = lax.all_gather(both, axis, axis=dim, tiled=True)
    return tuple(jnp.split(whole, [sum(widths[:k]) for k in range(1, len(widths))], axis=along))


def gather_turned(arrays, axis, dims):
    turned = [jnp.moveaxis(a, dim, 0) for a, dim in zip(arrays, dims)]
    widths = [t[0].size for t in turned]
    both = jnp.concatenate([t.reshape(-1, w) for t, w in zip(turned, widths)], axis=1)
    whole = lax.all_gather(both, axis, axis=0, tiled=True)
    parts = jnp.split(whole, [sum(widths[:k]) for k in range(1, len(widths))], axis=1)
    return tuple(
        (
            jnp.moveaxis(b.reshape(-1, *t.shape[1:]), 0, dim)
            for b, t, dim in zip(parts, turned, dims)
        )
    )


def summed_rows(x, axes, dim):
    if not axes:
        return x
    nearer = lax.psum_scatter(x, axes[0], scatter_dimension=dim, tiled=True)
    return summed_rows(nearer, axes[1:], dim)


def in_blocks(x, dim, peers):
    before, after = (x.shape[:dim], x.shape[dim + 1 :])
    return jnp.moveaxis(x.reshape(*before, peers, -1, *after), dim, 0)


def sum_at_owner(x, axis, dim):
    peers = lax.axis_size(axis)
    parts = lax.all_to_all(in_blocks(x, dim, peers), axis, 0, 0, tiled=True)
    return jnp.sum(parts.astype(jnp.float32), axis=0)


def copy_for_each(x, axis):
    peers = lax.axis_size(axis)
    return lax.all_to_all(jnp.broadcast_to(x[None], (peers, *x.shape)), axis, 0, 0, tiled=True)


def taken_together(x, axis):
    everything = copy_for_each(x, axis)
    return jnp.sum(everything, axis=0)


def in_one(arrays, axis):
    line, at, gathered = (jnp.concatenate([a.reshape(-1) for a in arrays]), 0, [])
    total = taken_together(line, axis)
    for a in arrays:
        gathered.append(total[at : at + a.size].reshape(a.shape))
        at += a.size
    return tuple(gathered)


def contract(left, right, left_dim, right_dim):
    return lax.dot_general(
        left, right, (((left_dim,), (right_dim,)), ((), ())), preferred_element_type=jnp.float32
    )


def rms_back(grad_rows, unit_rows, inv_rms, gain_rows):
    scaled = gain_rows * grad_rows
    inner = jnp.mean(scaled * unit_rows, axis=-1, keepdims=True)
    return inv_rms * (scaled - unit_rows * inner)


def on_device(tokens, grad_out, norm_gain, gate_weight, up_weight, down_weight):
    full_tokens, full_grad = sent_together((tokens, grad_out), "tp", 1, 0)
    floated = full_tokens.astype(jnp.float32)
    inv_rms = lax.rsqrt(jnp.mean(floated * floated, axis=-1, keepdims=True) + 1e-06)
    unit_rows = floated * inv_rms
    gain_rows = norm_gain[None, :]
    normed = (unit_rows * gain_rows).astype(jnp.bfloat16)
    gate_full, up_full, down_full = gather_turned(
        (gate_weight, up_weight, down_weight), FS, (1, 1, 1)
    )
    grad_hidden = 0.5 * contract(full_grad, down_full, 1, 1)
    factor = (full_tokens.shape[0] * lax.axis_size(FS)) ** (-0.5)
    gate_pre = contract(normed, gate_full, 1, 1)
    up_pre = contract(normed, up_full, 1, 1)
    sigma = jax.nn.sigmoid(gate_pre)
    active = gate_pre * sigma
    hidden = (active * up_pre).astype(jnp.bfloat16)
    term_down = 0.5 * factor * contract(hidden, full_grad, 0, 0)
    grad_down = summed_rows(term_down.astype(jnp.bfloat16), FS, 1).astype(jnp.float32)
    gate_grad_pre = (grad_hidden * up_pre * sigma * (1.0 + gate_pre * (1.0 - sigma))).astype(
        jnp.bfloat16
    )
    term_gate = factor * contract(gate_grad_pre, normed, 0, 0)
    grad_gate = summed_rows(term_gate.astype(jnp.bfloat16), FS, 1).astype(jnp.float32)
    up_grad_pre = (grad_hidden * active).astype(jnp.bfloat16)
    term_up = factor * contract(up_grad_pre, normed, 0, 0)
    grad_up = sum_at_owner(term_up.astype(jnp.bfloat16), FS, 1)
    grad_rows = jnp.dot(gate_grad_pre, gate_full, preferred_element_type=jnp.float32)
    grad_rows = grad_rows + jnp.dot(up_grad_pre, up_full, preferred_element_type=jnp.float32)
    partial_value = rms_back(grad_rows, unit_rows, inv_rms, gain_rows)
    summed = sum_at_owner(partial_value.astype(jnp.bfloat16), "tp", 1)
    grad_input = (grad_out.astype(jnp.float32) + summed).astype(jnp.bfloat16)
    width_total = gate_weight.shape[1] * lax.axis_size(FS)
    gate_rows, up_rows, down_rows = in_one(
        (
            jnp.sum(grad_gate * grad_gate, axis=1),
            jnp.sum(grad_up * grad_up, axis=1),
            jnp.sum(grad_down * grad_down, axis=1),
        ),
        FS,
    )
    row_squares = jnp.stack([gate_rows, up_rows, down_rows]) / width_total
    return (grad_input, grad_gate, grad_up, grad_down, row_squares)


def solution(mesh):
    split = Mesh(mesh.devices.reshape(8, 4, mesh.shape["tp"]), ("fs_0", "fs_1", "tp"))
    return jax.shard_map(
        on_device,
        mesh=split,
        in_specs=(P(FS, "tp"), P(FS, "tp"), P(), P("tp", FS), P("tp", FS), P("tp", FS)),
        out_specs=(P(FS, "tp"), P("tp", FS), P("tp", FS), P("tp", FS), P(None, "tp")),
        check_vma=False,
    )
```

profile of v0, /device:TPU:32, one launch (start us, length us, event | category | flops | bytes accessed | tf_op | source)
XLA Modules:
  0.0 352.2 jit_solution(1920257956523172577)
XLA Ops:
  7.2 0.0 all-gather.3.cloned.1.call-start
  7.2 2.3 pad_maximum_fusion
  9.5 0.0 all-gather.3.cloned.1.call-update
  9.5 0.0 all-gather.5.cloned.1.call-start
  9.6 1.5 pad_maximum_fusion.1
  11.1 0.0 all-gather.5.cloned.1.call-update
  11.1 0.0 reduce-scatter.11.cloned.1.call-start
  11.2 57.3 %all-gather.3.cloned.1.call-done = bf16[2048,2048]{1,0:T(8,128)(2,1)} async-done(((bf16[2048,256]{1,0:T(8,128)(2,1)}), bf16[2048,2048]{1,0:T(8,128)(2,1)}) %all-gather.3.cloned.1.call-update) | async-done | bytes 8388624 | tf_op jit(solution)/shard_map/all_gather | solution.py:13
  68.4 3.1 fusion.8
  71.5 83.8 %all-gather.5.cloned.1.call-done = bf16[2048,1152]{1,0:T(8,128)(2,1)} async-done(((bf16[64,1152]{1,0:T(8,128)(2,1)}), bf16[2048,1152]{1,0:T(8,128)(2,1)}) %all-gather.5.cloned.1.call-update) | async-done | bytes 4718608 | tf_op jit(solution)/shard_map/all_gather | solution.py:21
  155.3 5.2 %fusion.19 = f32[1024,384]{1,0:T(8,128)S(1)} fusion(bf16[2048,1152]{1,0:T(8,128)(2,1)} %all-gather.5.cloned.1.call-done, f32[2048]{0:T(1024)S(1)} %copy-done.2, f32[1024]{0:T(1024)S(1)} %add_rsqrt_fusion, bf16[2048,2048]{1,0:T(8,128)(2,1)} %all-gather.3.cloned.1.call-done), kind=kOutput, calls=%fused_computation.30 | convolution fusion | flops 1619001344 | bytes 7352320 | tf_op jit(solution)/shard_map/dot_general | solution.py:69
  160.5 5.2 %fusion.22 = f32[1024,384]{1,0:T(8,128)S(1)} fusion(bf16[2048,1152]{1,0:T(8,128)(2,1)} %all-gather.5.cloned.1.call-done, f32[2048]{0:T(1024)S(1)} %copy-done.2, f32[1024]{0:T(1024)S(1)} %add_rsqrt_fusion, bf16[2048,2048]{1,0:T(8,128)(2,1)} %all-gather.3.cloned.1.call-done), kind=kOutput, calls=%fused_computation.33 | convolution fusion | flops 1619001344 | bytes 7352320 | tf_op jit(solution)/shard_map/dot_general | solution.py:69
  165.7 3.1 multiply_convert_fusion
  168.8 0.0 reduce-scatter.11.cloned.1.call-update
  168.8 5.9 %multiply_convert_fusion.4 = (bf16[1024,384]{1,0:T(8,128)(2,1)S(1)}, bf16[1024,384]{1,0:T(8,128)(2,1)S(1)}) fusion(f32[1024,384]{1,0:T(8,128)S(1)} %fusion.19, f32[1024,384]{1,0:T(8,128)} %copy-done.3, bf16[2048,1152]{1,0:T(8,128)(2,1)} %all-gather.5.cloned.1.call-done, bf16[2048,2048]{1,0:T(8,128)(2,1)} %all-gather.3.cloned.1.call-done), kind=kOutput, calls=%fused_computation.24 | convolution fusion | flops 1616117760 | bytes 10485760 | tf_op jit(solution)/shard_map/dot_general | solution.py:69
  174.8 4.2 %multiply_convert_fusion.1 = bf16[384,2048]{1,0:T(8,128)(2,1)S(1)} fusion(bf16[1024,384]{1,0:T(8,128)(2,1)S(1)} %get-tuple-element.30, f32[2048]{0:T(1024)S(1)} %copy-done.2, f32[1024]{0:T(1024)S(1)} %add_rsqrt_fusion, bf16[2048,2048]{1,0:T(8,128)(2,1)} %all-gather.3.cloned.1.call-done), kind=kOutput, calls=%fused_computation.20 | convolution fusion | flops 1620574208 | bytes 6565888 | tf_op jit(solution)/shard_map/dot_general | solution.py:69
  179.0 1.6 copy.25
  180.5 6.2 %all-to-all-start.1 = ((bf16[32,384,64]{1,2,0:T(8,128)(2,1)}), bf16[32,384,64]{1,2,0:T(8,128)(2,1)S(1)}, u32[]{:S(2)}, u32[]{:S(2)}) async-start(bf16[32,384,64]{1,2,0:T(8,128)(2,1)} %bitcast.5), calls=%async_computation.2 | async-start | bytes 3145728 | tf_op jit(solution)/shard_map/all_to_all | solution.py:45
  186.8 0.2 reduce-scatter.9.cloned.1.call-start
  187.0 5.4 %multiply_convert_fusion.2 = bf16[384,2048]{1,0:T(8,128)(2,1)} fusion(bf16[1024,384]{1,0:T(8,128)(2,1)S(1)} %get-tuple-element.31, f32[2048]{0:T(1024)S(1)} %copy-done.2, f32[1024]{0:T(1024)S(1)} %add_rsqrt_fusion, bf16[2048,2048]{1,0:T(8,128)(2,1)} %all-gather.3.cloned.1.call-done), kind=kOutput, calls=%fused_computation.21 | convolution fusion | flops 1620574208 | bytes 6565888 | tf_op jit(solution)/shard_map/dot_general | solution.py:69
  192.4 3.9 %fusion.17 = f32[1024,2048]{1,0:T(8,128)S(1)} fusion(bf16[1024,384]{1,0:T(8,128)(2,1)S(1)} %get-tuple-element.31, bf16[2048,1152]{1,0:T(8,128)(2,1)} %all-gather.5.cloned.1.call-done), kind=kOutput, calls=%fused_computation.28 | convolution fusion | flops 1610612736 | bytes 10747904 | tf_op jit(solution)/shard_map/dot_general | solution.py:107
  196.3 5.6 %fusion.4 = (f32[1024]{0:T(1024)S(1)}, f32[1024,2048]{1,0:T(8,128)S(1)}) fusion(f32[1024]{0:T(1024)S(1)} %add_rsqrt_fusion, bf16[2048,2048]{1,0:T(8,128)(2,1)} %all-gather.3.cloned.1.call-done, f32[1024,2048]{1,0:T(8,128)S(1)} %fusion.17, bf16[1024,384]{1,0:T(8,128)(2,1)S(1)} %get-tuple-element.30, bf16[2048,1152]{1,0:T(8,128)(2,1)} %all-gather.5.cloned.1.call-done, ...), kind=kOutput, calls=%fused_computation.6 | convolution fusion | flops 1623194624 | bytes 23347200 | tf_op jit(solution)/shard_map/dot_general | solution.py:108
  202.0 1.8 fusion.7
  203.9 2.2 copy.39
  206.1 26.4 %all-to-all-done.1 = bf16[32,384,64]{1,2,0:T(8,128)(2,1)S(1)} async-done(((bf16[32,384,64]{1,2,0:T(8,128)(2,1)}), bf16[32,384,64]{1,2,0:T(8,128)(2,1)S(1)}, u32[]{:S(2)}, u32[]{:S(2)}) %all-to-all-start.1) | async-done | bytes 1572896 | tf_op jit(solution)/shard_map/all_to_all | solution.py:45
  232.5 4.6 %all-to-all-start = ((bf16[8,1024,256]{2,1,0:T(8,128)(2,1)}), bf16[8,1024,256]{2,1,0:T(8,128)(2,1)}, u32[]{:S(2)}, u32[]{:S(2)}) async-start(bf16[8,1024,256]{2,1,0:T(8,128)(2,1)} %bitcast.25), calls=%async_computation | async-start | bytes 8388608 | tf_op jit(solution)/shard_map/all_to_all | solution.py:45
  237.0 0.0 reduce-scatter.15.cloned.1.call-start
  237.1 0.0 reduce-scatter.11.cloned.1.call-done
  237.1 1.7 copy.31
  238.9 0.0 reduce-scatter.15.cloned.1.call-update
  238.9 0.0 reduce-scatter.13.cloned.1.call-start
  238.9 33.6 %reduce-scatter.9.cloned.1.call-done = bf16[384,256]{1,0:T(8,128)(2,1)} async-done(((bf16[384,2048]{1,0:T(8,128)(2,1)}), bf16[384,256]{1,0:T(8,128)(2,1)}) %reduce-scatter.9.cloned.1.call-update) | async-done | bytes 196624 | tf_op jit(solution)/shard_map/reduce_scatter | solution.py:34
  272.6 1.7 copy.29
  274.3 0.2 convert_reduce_fusion.1
  274.6 23.1 %reduce-scatter.15.cloned.1.call-done = bf16[64,384]{1,0:T(8,128)(2,1)} async-done(((bf16[256,384]{1,0:T(8,128)(2,1)}), bf16[64,384]{1,0:T(8,128)(2,1)}) %reduce-scatter.15.cloned.1.call-update) | async-done | bytes 49168
  297.7 0.9 copy.32
  298.6 0.7 copy.28
  299.3 24.4 %reduce-scatter.13.cloned.1.call-done = bf16[64,384]{1,0:T(8,128)(2,1)} async-done(((bf16[256,384]{1,0:T(8,128)(2,1)}), bf16[64,384]{1,0:T(8,128)(2,1)}) %reduce-scatter.13.cloned.1.call-update) | async-done | bytes 49168
  323.7 0.9 copy.30
  324.6 0.7 copy.27
  325.3 0.2 multiply_reduce_fusion
  325.5 0.7 broadcast_in_dim.2
  326.3 8.5 %all-to-all-start.2 = ((f32[32,1,1152]{2,1,0:T(1,128)}), f32[32,1,1152]{2,1,0:T(1,128)S(1)}, u32[]{:S(2)}, u32[]{:S(2)}) async-start(f32[32,1,1152]{2,1,0:T(1,128)} %broadcast_in_dim.2), calls=%async_computation.4 | async-start | bytes 294912 | tf_op jit(solution)/shard_map/all_to_all | solution.py:51
  334.8 2.9 convert_reduce_fusion
  337.7 0.9 add_convert_fusion
  338.6 6.0 %all-to-all-done.2 = f32[32,1,1152]{2,1,0:T(1,128)S(1)} async-done(((f32[32,1,1152]{2,1,0:T(1,128)}), f32[32,1,1152]{2,1,0:T(1,128)S(1)}, u32[]{:S(2)}, u32[]{:S(2)}) %all-to-all-start.2) | async-done | bytes 147488 | tf_op jit(solution)/shard_map/all_to_all | solution.py:51
  344.6 0.1 reduce_sum.79
  344.7 0.6 maximum_multiply_fusion
  (29 shorter events, 0.1 us)
Async XLA Ops:
  7.2 148.1 %copy-start.2 = (f32[2048]{0:T(1024)S(1)}, f32[2048]{0:T(1024)}, u32[]{:S(2)}) copy-start(f32[2048]{0:T(1024)} %param.8) | copy-start | bytes 24580
  7.2 61.2 %all-gather.3.cloned.1.call-start = ((), (), s32[]{:S(2)}) async-start(), calls=%async_computation.7 | async-start | bytes 9437184 | tf_op jit(solution)/shard_map/all_gather | solution.py:13
  9.5 145.8 %all-gather.5.cloned.1.call-start = ((), (), s32[]{:S(2)}) async-start(), calls=%async_computation.8 | async-start | bytes 4866048 | tf_op jit(solution)/shard_map/all_gather | solution.py:21
  11.1 226.0 %reduce-scatter.11.cloned.1.call-start = ((), (), s32[]{:S(2)}) async-start(), calls=%async_computation.10 | async-start | bytes 1769472 | tf_op jit(solution)/shard_map/reduce_scatter | solution.py:34
  155.3 10.4 %slice-start = ((s8[8388608]{0:T(1024)(128)(4,1)}), s8[4194304]{0:T(1024)(128)(4,1)S(1)}, s32[]{:S(2)}) async-start(s8[8388608]{0:T(1024)(128)(4,1)} %bitcast.21), calls=%async_computation.13 | async-start | bytes 8388608
  160.5 5.2 %slice-start.1 = ((s8[8388608]{0:T(1024)(128)(4,1)}), s8[4194304]{0:T(1024)(128)(4,1)S(1)}, s32[]{:S(2)}) async-start(s8[8388608]{0:T(1024)(128)(4,1)} %bitcast.21), calls=%async_computation.14 | async-start | bytes 8388608
  165.7 3.1 copy-start.3
  180.5 51.9 %all-to-all-start.1 = ((bf16[32,384,64]{1,2,0:T(8,128)(2,1)}), bf16[32,384,64]{1,2,0:T(8,128)(2,1)S(1)}, u32[]{:S(2)}, u32[]{:S(2)}) async-start(bf16[32,384,64]{1,2,0:T(8,128)(2,1)} %bitcast.5), calls=%async_computation.2 | async-start | bytes 3145728 | tf_op jit(solution)/shard_map/all_to_all | solution.py:45
  186.8 85.8 %reduce-scatter.9.cloned.1.call-start = ((), (), s32[]{:S(2)}) async-start(), calls=%async_computation.9 | async-start | bytes 1769472 | tf_op jit(solution)/shard_map/reduce_scatter | solution.py:34
  192.4 9.6 %slice-start.2 = ((s8[8388608]{0:T(1024)(128)(4,1)}), s8[4194304]{0:T(1024)(128)(4,1)S(1)}, s32[]{:S(2)}) async-start(s8[8388608]{0:T(1024)(128)(4,1)} %bitcast.23), calls=%async_computation.15 | async-start | bytes 8388608
  196.3 5.7 %slice-start.3 = ((s8[8388608]{0:T(1024)(128)(4,1)}), s8[4194304]{0:T(1024)(128)(4,1)S(1)}, s32[]{:S(2)}) async-start(s8[8388608]{0:T(1024)(128)(4,1)} %bitcast.23), calls=%async_computation.16 | async-start | bytes 8388608
  232.5 93.0 %all-to-all-start = ((bf16[8,1024,256]{2,1,0:T(8,128)(2,1)}), bf16[8,1024,256]{2,1,0:T(8,128)(2,1)}, u32[]{:S(2)}, u32[]{:S(2)}) async-start(bf16[8,1024,256]{2,1,0:T(8,128)(2,1)} %bitcast.25), calls=%async_computation | async-start | bytes 8388608 | tf_op jit(solution)/shard_map/all_to_all | solution.py:45
  237.0 60.6 %reduce-scatter.15.cloned.1.call-start = ((), (), s32[]{:S(2)}) async-start(), calls=%async_computation.12 | async-start | bytes 245760
  238.9 84.8 %reduce-scatter.13.cloned.1.call-start = ((), (), s32[]{:S(2)}) async-start(), calls=%async_computation.11 | async-start | bytes 245760
  274.3 63.3 %copy-start = (bf16[1024,256]{1,0:T(8,128)(2,1)S(1)}, bf16[1024,256]{1,0:T(8,128)(2,1)}, u32[]{:S(2)}) copy-start(bf16[1024,256]{1,0:T(8,128)(2,1)} %param.7) | copy-start | bytes 1572868
  274.6 64.0 %copy-start.1 = (f32[384,64]{0,1:T(8,128)}, f32[384,64]{0,1:T(8,128)S(1)}, u32[]{:S(2)}) copy-start(f32[384,64]{0,1:T(8,128)S(1)} %convert_reduce_fusion.1) | copy-start | bytes 294916
  326.3 18.3 %all-to-all-start.2 = ((f32[32,1,1152]{2,1,0:T(1,128)}), f32[32,1,1152]{2,1,0:T(1,128)S(1)}, u32[]{:S(2)}, u32[]{:S(2)}) async-start(f32[32,1,1152]{2,1,0:T(1,128)} %broadcast_in_dim.2), calls=%async_computation.4 | async-start | bytes 294912 | tf_op jit(solution)/shard_map/all_to_all | solution.py:51
Sparse Core Ops, SparseCore 0:
  9.8 58.5 all-gather.2
  71.6 83.6 all-gather.4
  169.0 54.1 reduce-scatter.10
  225.6 46.8 reduce-scatter.8
  274.9 22.6 reduce-scatter.14
  300.6 23.0 reduce-scatter.12
where the time goes:
time: 354 us; the launch traced here: 352 us
  waiting for transfers between devices  255 us (72%)
  matrix products  38.5 us (11%)
  starting transfers between devices  19.7 us (6%)
  between operations  14.4 us (4%)
  other arithmetic  13.6 us (4%)
  local copies, waits for them, and re-layouts  11.4 us (3%)
    all_gather x1, waiting for transfers between devices, gather_turned(): whole = lax.all_gather(both, axis, axis=0, tiled=True)  83.8 us
    all_gather x1, waiting for transfers between devices, sent_together(): whole = lax.all_gather(both, axis, axis=dim, tiled=True)  57.3 us
    unnamed x8, waiting for transfers between devices  47.5 us
    reduce_scatter x2, waiting for transfers between devices, summed_rows(): nearer = lax.psum_scatter(x, axes[0], scatter_dimension=dim, tiled=True)  33.7 us
    dot_general x6, matrix products, contract(): lax.dot_general(left, right, (((left_dim,), (right_dim,)), ((), ())), pre...  29 us
    all_to_all x2, waiting for transfers between devices, sum_at_owner(): parts = lax.all_to_all(in_blocks(x, dim, peers), axis, 0, 0, tiled=True)  26.4 us
    all_to_all x2, starting transfers between devices, sum_at_owner(): parts = lax.all_to_all(in_blocks(x, dim, peers), axis, 0, 0, tiled=True)  10.8 us
    all_to_all x1, starting transfers between devices, copy_for_each(): lax.all_to_all(jnp.broadcast_to(x[None], (peers, *x.shape)), axis, 0, 0,...  8.54 us
  transfers between devices with their start and end apart: 9, of which 7 were waited for; matrix products, arithmetic and copies ran while one was open for 13% of the time, Pallas kernels for 0%

commit v1 on v0

v1 whole, which is shorter than its diff:
```python
import jax
import jax.numpy as jnp
from jax import lax
from jax.experimental import pallas as pl
from jax.experimental.pallas import tpu as pltpu
from jax.sharding import Mesh
from jax.sharding import PartitionSpec as P

FS = ("z", "x")
TP = ("y", "c")
NZ, NX, NY, NC = 8, 4, 4, 2
F32, BF16 = jnp.float32, jnp.bfloat16
CHUNKS = 4
COPIES = 184
ORDER = (4, 3, -3, 2, -2, 1, -1, 0)


class Net:
    def __init__(self, send_sems, recv_sems):
        self.send_sems, self.recv_sems, self.copies = send_sems, recv_sems, []

    def send(self, src, dst, **to):
        at = len(self.copies)
        copy = pltpu.make_async_remote_copy(
            src_ref=src,
            dst_ref=dst,
            send_sem=self.send_sems.at[at],
            recv_sem=self.recv_sems.at[at],
            device_id=to,
            device_id_type=pl.DeviceIdType.MESH,
        )
        copy.start()
        self.copies.append(copy)
        return copy

    def finish(self):
        for copy in self.copies:
            copy.wait_send()


def lanes_summed(v):
    total = v[:, 0:128]
    for at in range(128, v.shape[1], 128):
        total = total + v[:, at : at + 128]
    return total


def turned(left, right):
    return lax.dot_general(left, right, (((0,), (0,)), ((), ())), preferred_element_type=F32)


def kernel(
    tok, grd, gain, wgu, wdn,
    out_in, out_gu, out_dn, out_sq,
    T, G, N, GU, DN, AB, H, INV, V, DGU, DDN,
    SX1, RX1, SX2, RX2, XR, SZ, RZ, SD, RD, FD, SE1, RE1, SE2, RE2,
    PP, PR, S1, R1, S2, R2, QX, QZ,
    send_sems, recv_sems, local_sems,
):
    z, x, y, c = (lax.axis_index(a) for a in ("z", "x", "y", "c"))
    zz = lambda d: lax.rem(z + (d + NZ), NZ)
    xx = lambda d: lax.rem(x + (d + NX), NX)
    yy = lambda d: lax.rem(y + (d + NY), NY)
    other = 1 - c
    me = y * NC + c
    slot = lambda d: yy(d) * NC + c
    tokens = tok.shape[0]
    rows = tokens // CHUNKS
    wide = tok.shape[1]
    ff = wdn.shape[1]
    model = wide * NY * NC
    part = wgu.shape[0]
    half_part, half_rows = part // 2, rows // 2
    gate, up = pl.ds(0, ff), pl.ds(ff, ff)
    factor = (tokens * NZ * NX) ** (-0.5)
    span = lambda ch: pl.ds(ch * rows, rows)

    barrier = pltpu.get_barrier_semaphore()
    peers = [{"z": zz(d)} for d in range(1, NZ)] + [{"x": xx(d)} for d in range(1, NX)]
    peers += [{"y": yy(1)}, {"y": yy(-1)}, {"c": other}]
    for peer in peers:
        pl.semaphore_signal(barrier, inc=1, device_id=peer, device_id_type=pl.DeviceIdType.MESH)
    locals_ = [
        pltpu.make_async_copy(src, dst, local_sems.at[i])
        for i, (src, dst) in enumerate(
            ((wgu, GU.at[z, x]), (wdn, DN.at[z, x]), (tok, T.at[me]), (grd, G.at[me]))
        )
    ]
    for copy in locals_:
        copy.start()
    pl.semaphore_wait(barrier, len(peers))
    net = Net(send_sems, recv_sems)

    gz, gx, gxf, dx, dxf, dz, ya, yb, dd = {}, {}, {}, {}, {}, {}, {}, {}, {}

    def gx_send(d, src):
        gx[d, 1] = net.send(src, GU.at[zz(d), x], x=xx(1))
        gx[d, -1] = net.send(src, GU.at[zz(d), x], x=xx(-1))

    def gx_pass(d):
        gx[d, 1].wait_recv()
        ref = GU.at[zz(d), xx(-1), :, gate]
        gxf[d, 1] = net.send(ref, ref, x=xx(1))
        gx[d, -1].wait_recv()
        ref = GU.at[zz(d), xx(1), :, up]
        gxf[d, -1] = net.send(ref, ref, x=xx(-1))

    def gz_step(s):
        for way in (1, -1):
            gz[s, way].wait_recv()
            if s < NZ // 2:
                ref = GU.at[zz(-way * s), x]
                if s == NZ // 2 - 1:
                    ref = GU.at[zz(-way * s), x, :, gate if way == 1 else up]
                gz[s + 1, way] = net.send(ref, ref, z=zz(way))
        if s < NZ // 2:
            gx_send(-s, GU.at[zz(-s), x])
            gx_send(s, GU.at[zz(s), x])
        else:
            gx_send(s, GU.at[zz(s), x])

    def dx_pass():
        dx[1].wait_recv()
        ref = DN.at[z, xx(-1), pl.ds(0, half_part)]
        dxf[1] = net.send(ref, ref, x=xx(1))
        dx[-1].wait_recv()
        ref = DN.at[z, xx(1), pl.ds(half_part, half_part)]
        dxf[-1] = net.send(ref, ref, x=xx(-1))

    def dz_step(s):
        for way in (1, -1):
            if s == 0:
                ref = DN.at[z]
            else:
                dz[s, way].wait_recv()
                ref = DN.at[zz(-way * s)]
                if s == NZ // 2 - 1:
                    ref = DN.at[zz(-way * s), pl.ds(0 if way == 1 else NX // 2, NX // 2)]
            if s < NZ // 2:
                dz[s + 1, way] = net.send(ref, ref, z=zz(way))

    def y_own(ch):
        for way in (1, -1):
            ya["T", ch, way] = net.send(tok.at[span(ch)], T.at[me, span(ch)], y=yy(way))
            ya["G", ch, way] = net.send(grd.at[span(ch)], G.at[me, span(ch)], y=yy(way))

    def to_other(name, full, d, ch):
        ref = full.at[slot(d), span(ch)]
        dd[name, d, ch] = net.send(ref, ref, c=other)

    def y_pass(ch):
        ya["T", ch, 1].wait_recv()
        ref = T.at[slot(-1), span(ch)]
        yb["T", ch] = net.send(ref, ref, y=yy(1))
        to_other("T", T, -1, ch)
        ya["G", ch, -1].wait_recv()
        ref = G.at[slot(1), span(ch)]
        yb["G", ch] = net.send(ref, ref, y=yy(-1))
        to_other("G", G, 1, ch)
        ya["G", ch, 1].wait_recv()
        to_other("G", G, -1, ch)
        ya["T", ch, -1].wait_recv()
        to_other("T", T, 1, ch)

    def y_last(ch):
        yb["T", ch].wait_recv()
        to_other("T", T, 2, ch)
        yb["G", ch].wait_recv()
        to_other("G", G, 2, ch)

    def y_ready(ch):
        if ch == 0:
            dd["T"].wait_recv()
            dd["G"].wait_recv()
            locals_[2].wait()
            locals_[3].wait()
        for d in (-1, 1, 2):
            dd["T", d, ch].wait_recv()
            dd["G", d, ch].wait_recv()

    def norm(ch):
        total = jnp.zeros((rows, 128), F32)
        for k in range(NY * NC):
            t = T[k, span(ch)].astype(F32)
            total = total + lanes_summed(t * t)
        inv = lax.rsqrt(jnp.sum(total, axis=1, keepdims=True) / model + 1e-06)
        INV[span(ch)] = inv
        for k in range(NY * NC):
            t = T[k, span(ch)].astype(F32)
            N[k, span(ch)] = (t * inv * gain[k]).astype(BF16)

    def forward(ch):
        pre = jnp.zeros((rows, 2 * ff), F32)
        gh = jnp.zeros((rows, ff), F32)
        for k in range(NY * NC):
            pre = pre + jnp.dot(
                N[k, span(ch)], GU[k].reshape(wide, 2 * ff), preferred_element_type=F32
            )
            gh = gh + jnp.dot(G[k, span(ch)], DN[k].reshape(wide, ff), preferred_element_type=F32)
        gh = 0.5 * gh
        g, u = pre[:, 0:ff], pre[:, ff : 2 * ff]
        sigma = jax.nn.sigmoid(g)
        active = g * sigma
        H[span(ch)] = (active * u).astype(BF16)
        AB[span(ch), 0:ff] = (gh * u * sigma * (1.0 + g * (1.0 - sigma))).astype(BF16)
        AB[span(ch), ff : 2 * ff] = (gh * active).astype(BF16)

    def weights(d):
        k = zz(d)
        DGU[k] = (factor * turned(N[k], AB[...])).reshape(NX, part, 2 * ff)
        DDN[k] = (0.5 * factor * turned(G[k], H[...])).reshape(NX, part, ff)

    def partial(ch):
        ab = AB[span(ch)]
        inv = INV[span(ch)]
        total = jnp.zeros((rows, 128), F32)
        for k in range(NY * NC):
            v = gain[k] * lax.dot_general(
                ab,
                GU[k].reshape(wide, 2 * ff),
                (((1,), (1,)), ((), ())),
                preferred_element_type=F32,
            )
            V[k] = v
            total = total + lanes_summed(v * (T[k, span(ch)].astype(F32) * inv))
        inner = jnp.sum(total, axis=1, keepdims=True) / model
        for k in range(NY * NC):
            unit = T[k, span(ch)].astype(F32) * inv
            PP[k % NC, k // NC, span(ch)] = (inv * (V[k] - unit * inner)).astype(BF16)

    x1, x2, zs, ds, e1, e2, pc, p1, p2 = {}, {}, {}, {}, {}, {}, {}, {}, {}

    def x_step1(i):
        k = zz(ORDER[i])
        SX1[i, 0] = DGU[k, xx(2), :, gate].astype(BF16)
        SX1[i, 1] = DGU[k, xx(2), :, up].astype(BF16)
        x1[i, 1] = net.send(SX1.at[i, 0], RX1.at[i, 0], x=xx(1))
        x1[i, -1] = net.send(SX1.at[i, 1], RX1.at[i, 1], x=xx(-1))

    def x_step2(i):
        k = zz(ORDER[i])
        x1[i, 1].wait_recv()
        SX2[i, 0, :, gate] = (DGU[k, xx(1), :, gate] + RX1[i, 0].astype(F32)).astype(BF16)
        SX2[i, 0, :, up] = DGU[k, xx(1), :, up].astype(BF16)
        x2[i, 1] = net.send(SX2.at[i, 0], RX2.at[i, 0], x=xx(1))
        x1[i, -1].wait_recv()
        SX2[i, 1, :, gate] = DGU[k, xx(-1), :, gate].astype(BF16)
        SX2[i, 1, :, up] = (DGU[k, xx(-1), :, up] + RX1[i, 1].astype(F32)).astype(BF16)
        x2[i, -1] = net.send(SX2.at[i, 1], RX2.at[i, 1], x=xx(-1))

    def x_sum(i):
        x2[i, 1].wait_recv()
        x2[i, -1].wait_recv()
        return DGU[zz(ORDER[i]), x] + RX2[i, 0].astype(F32) + RX2[i, 1].astype(F32)

    def z_step(i):
        d = ORDER[i]
        value = x_sum(i)
        if d == NZ // 2:
            SZ[0, 0] = value.astype(BF16)
            zs[1, d] = net.send(SZ.at[0, 0, :, gate], RZ.at[0, 0, :, gate], z=zz(1))
            zs[-1, d] = net.send(SZ.at[0, 0, :, up], RZ.at[0, 1, :, up], z=zz(-1))
            return None
        ways = (1, -1) if d == 0 else (1 if d > 0 else -1,)
        for way in ways:
            s, w = NZ // 2 - abs(d), 0 if way == 1 else 1
            zs[way, abs(d) + 1].wait_recv()
            if s == 1:
                cols = gate if way == 1 else up
                XR[...] = value
                XR[:, cols] = XR[:, cols] + RZ[0, w, :, cols].astype(F32)
                value = XR[...]
            else:
                value = value + RZ[s - 1, w].astype(F32)
            if d != 0:
                SZ[s, w] = value.astype(BF16)
                zs[way, abs(d)] = net.send(SZ.at[s, w], RZ.at[s, w], z=zz(way))
        return value

    def d_step(i):
        d = ORDER[i]
        k = zz(d)
        near = NX // 2
        if d == NZ // 2:
            SD[0, 0] = DDN[k].astype(BF16)
            lo, hi = pl.ds(0, near), pl.ds(near, near)
            ds[1, d] = net.send(SD.at[0, 0, lo], RD.at[0, 0, lo], z=zz(1))
            ds[-1, d] = net.send(SD.at[0, 0, hi], RD.at[0, 1, hi], z=zz(-1))
            return
        if d == 0:
            ds[1, 1].wait_recv()
            ds[-1, 1].wait_recv()
            last = NZ // 2 - 1
            FD[...] = DDN[k] + RD[last, 0].astype(F32) + RD[last, 1].astype(F32)
            return
        way = 1 if d > 0 else -1
        s, w = NZ // 2 - abs(d), 0 if way == 1 else 1
        ds[way, abs(d) + 1].wait_recv()
        if s == 1:
            own = pl.ds(near if way == 1 else 0, near)
            sent = pl.ds(0 if way == 1 else near, near)
            SD[s, w, own] = DDN[k, own].astype(BF16)
            SD[s, w, sent] = (DDN[k, sent] + RD[0, w, sent].astype(F32)).astype(BF16)
        else:
            SD[s, w] = (DDN[k] + RD[s - 1, w].astype(F32)).astype(BF16)
        ds[way, abs(d)] = net.send(SD.at[s, w], RD.at[s, w], z=zz(way))

    def e_step1():
        SE1[...] = FD[xx(2)].astype(BF16)
        lo, hi = pl.ds(0, half_part), pl.ds(half_part, half_part)
        e1[1] = net.send(SE1.at[lo], RE1.at[lo], x=xx(1))
        e1[-1] = net.send(SE1.at[hi], RE1.at[hi], x=xx(-1))

    def e_step2():
        lo, hi = pl.ds(0, half_part), pl.ds(half_part, half_part)
        e1[1].wait_recv()
        SE2[0, lo] = (FD[xx(1), lo] + RE1[lo].astype(F32)).astype(BF16)
        SE2[0, hi] = FD[xx(1), hi].astype(BF16)
        e2[1] = net.send(SE2.at[0], RE2.at[0], x=xx(1))
        e1[-1].wait_recv()
        SE2[1, lo] = FD[xx(-1), lo].astype(BF16)
        SE2[1, hi] = (FD[xx(-1), hi] + RE1[hi].astype(F32)).astype(BF16)
        e2[-1] = net.send(SE2.at[1], RE2.at[1], x=xx(-1))

    def e_sum():
        e2[1].wait_recv()
        e2[-1].wait_recv()
        return FD[x] + RE2[0].astype(F32) + RE2[1].astype(F32)

    def p_send(ch):
        pc[ch] = net.send(PP.at[other, :, span(ch)], PR.at[:, span(ch)], c=other)

    def p_pair(ch, d, at, n):
        sub = pl.ds(ch * rows + at, n)
        return PP[c, yy(d), sub].astype(F32) + PR[yy(d), sub].astype(F32)

    def p_step1(ch):
        pc[ch].wait_recv()
        S1[ch] = p_pair(ch, 2, 0, rows).astype(BF16)
        lo, hi = pl.ds(0, half_rows), pl.ds(half_rows, half_rows)
        p1[ch, 1] = net.send(S1.at[ch, lo], R1.at[ch, lo], y=yy(1))
        p1[ch, -1] = net.send(S1.at[ch, hi], R1.at[ch, hi], y=yy(-1))

    def p_step2(ch):
        lo, hi = pl.ds(0, half_rows), pl.ds(half_rows, half_rows)
        p1[ch, 1].wait_recv()
        S2[ch, 0, lo] = (p_pair(ch, 1, 0, half_rows) + R1[ch, lo].astype(F32)).astype(BF16)
        S2[ch, 0, hi] = p_pair(ch, 1, half_rows, half_rows).astype(BF16)
        p2[ch, 1] = net.send(S2.at[ch, 0], R2.at[ch, 0], y=yy(1))
        p1[ch, -1].wait_recv()
        S2[ch, 1, lo] = p_pair(ch, -1, 0, half_rows).astype(BF16)
        S2[ch, 1, hi] = (
            p_pair(ch, -1, half_rows, half_rows) + R1[ch, hi].astype(F32)
        ).astype(BF16)
        p2[ch, -1] = net.send(S2.at[ch, 1], R2.at[ch, 1], y=yy(-1))

    def p_sum(ch):
        p2[ch, 1].wait_recv()
        p2[ch, -1].wait_recv()
        total = p_pair(ch, 0, 0, rows) + R2[ch, 0].astype(F32) + R2[ch, 1].astype(F32)
        out_in[span(ch)] = (grd[span(ch)].astype(F32) + total).astype(BF16)

    for way in (1, -1):
        gz[1, way] = net.send(wgu, GU.at[z, x], z=zz(way))
        dx[way] = net.send(wdn, DN.at[z, x], x=xx(way))
    gx_send(0, wgu)
    y_own(0)
    dd["T"] = net.send(tok, T.at[me], c=other)
    dd["G"] = net.send(grd, G.at[me], c=other)
    y_own(1)
    locals_[0].wait()
    locals_[1].wait()
    dx_pass()
    gz_step(1)
    gx_pass(0)
    dxf[1].wait_recv()
    dxf[-1].wait_recv()
    dz_step(0)
    y_pass(0)
    y_own(2)
    gz_step(2)
    gx_pass(-1)
    gx_pass(1)
    dz_step(1)
    y_pass(1)
    y_own(3)
    gz_step(3)
    gx_pass(-2)
    gx_pass(2)
    dz_step(2)
    y_last(0)
    y_ready(0)
    norm(0)
    gz_step(4)
    y_pass(2)
    gx_pass(-3)
    gx_pass(3)
    dz_step(3)
    y_last(1)
    y_ready(1)
    norm(1)
    gx_pass(4)
    y_pass(3)
    dz_step(4)
    for d in (0, -1, 1, -2, 2, -3, 3, 4):
        gxf[d, 1].wait_recv()
        gxf[d, -1].wait_recv()
    forward(0)
    y_last(2)
    y_ready(2)
    norm(2)
    forward(1)
    y_last(3)
    y_ready(3)
    norm(3)
    forward(2)
    forward(3)

    steps = len(ORDER)
    for i in range(steps):
        weights(ORDER[i])
        x_step1(i)
        d_step(i)
        if i >= 1:
            x_step2(i - 1)
        if i % 2 == 0:
            partial(i // 2)
            p_send(i // 2)
        else:
            p_step1(i // 2)
            if i >= 3:
                p_step2(i // 2 - 1)
        if i >= 2:
            z_step(i - 2)
    x_step2(steps - 1)
    e_step1()
    p_step2(CHUNKS - 1)
    z_step(steps - 2)
    e_step2()
    for ch in range(CHUNKS - 1):
        p_sum(ch)
    down = e_sum()
    out_dn[...] = down
    both = z_step(steps - 1)
    out_gu[...] = both
    p_sum(CHUNKS - 1)

    squares = jnp.concatenate(
        [jnp.sum(both * both, axis=0, keepdims=True), jnp.sum(down * down, axis=0, keepdims=True)],
        axis=1,
    )
    QX[x] = squares
    sent = [net.send(QX.at[x], QX.at[x], x=xx(d)) for d in range(1, NX)]
    for copy in sent:
        copy.wait_recv()
    total = QX[0]
    for at in range(1, NX):
        total = total + QX[at]
    QZ[z] = total
    sent = [net.send(QZ.at[z], QZ.at[z], z=zz(d)) for d in range(1, NZ)]
    for copy in sent:
        copy.wait_recv()
    total = QZ[0]
    for at in range(1, NZ):
        total = total + QZ[at]
    out_sq[...] = total / model
    assert len(net.copies) == COPIES, len(net.copies)
    net.finish()


def on_device(tokens, grad_out, norm_gain, gate_weight, up_weight, down_weight):
    n, wide = tokens.shape
    ff, part = gate_weight.shape
    blocks = NY * NC
    rows = n // CHUNKS
    wgu = jnp.concatenate([gate_weight, up_weight], axis=0).T
    wdn = down_weight.T
    gain = norm_gain.reshape(blocks, 1, wide)
    vm = pl.BlockSpec(memory_space=pltpu.VMEM)
    half = NZ // 2
    scratch = [
        ((blocks, n, wide), BF16),
        ((blocks, n, wide), BF16),
        ((blocks, n, wide), BF16),
        ((NZ, NX, part, 2 * ff), BF16),
        ((NZ, NX, part, ff), BF16),
        ((n, 2 * ff), BF16),
        ((n, ff), BF16),
        ((n, 1), F32),
        ((blocks, rows, wide), F32),
        ((NZ, NX, part, 2 * ff), F32),
        ((NZ, NX, part, ff), F32),
        ((NZ, 2, part, ff), BF16),
        ((NZ, 2, part, ff), BF16),
        ((NZ, 2, part, 2 * ff), BF16),
        ((NZ, 2, part, 2 * ff), BF16),
        ((part, 2 * ff), F32),
        ((half, 2, part, 2 * ff), BF16),
        ((half, 2, part, 2 * ff), BF16),
        ((half, 2, NX, part, ff), BF16),
        ((half, 2, NX, part, ff), BF16),
        ((NX, part, ff), F32),
        ((part, ff), BF16),
        ((part, ff), BF16),
        ((2, part, ff), BF16),
        ((2, part, ff), BF16),
        ((NC, NY, n, wide), BF16),
        ((NY, n, wide), BF16),
        ((CHUNKS, rows, wide), BF16),
        ((CHUNKS, rows, wide), BF16),
        ((CHUNKS, 2, rows, wide), BF16),
        ((CHUNKS, 2, rows, wide), BF16),
        ((NX, 1, 3 * ff), F32),
        ((NZ, 1, 3 * ff), F32),
    ]
    grad_in, grad_gu, grad_dn, squares = pl.pallas_call(
        kernel,
        out_shape=(
            jax.ShapeDtypeStruct((n, wide), BF16),
            jax.ShapeDtypeStruct((part, 2 * ff), F32),
            jax.ShapeDtypeStruct((part, ff), F32),
            jax.ShapeDtypeStruct((1, 3 * ff), F32),
        ),
        in_specs=[vm] * 5,
        out_specs=(vm,) * 4,
        scratch_shapes=[pltpu.VMEM(shape, dtype) for shape, dtype in scratch]
        + [
            pltpu.SemaphoreType.DMA((COPIES,)),
            pltpu.SemaphoreType.DMA((COPIES,)),
            pltpu.SemaphoreType.DMA((4,)),
        ],
        compiler_params=pltpu.CompilerParams(
            collective_id=0, has_side_effects=True, vmem_limit_bytes=67043328
        ),
        name="ffn_backward",
    )(tokens, grad_out, gain, wgu, wdn)
    return (
        grad_in,
        grad_gu[:, :ff].T,
        grad_gu[:, ff:].T,
        grad_dn.T,
        squares.reshape(3, ff),
    )


def solution(mesh):
    split = Mesh(mesh.devices.reshape(NZ, NX, NY, NC), FS + TP)
    return jax.shard_map(
        on_device,
        mesh=split,
        in_specs=(P(FS, TP), P(FS, TP), P(), P(TP, FS), P(TP, FS), P(TP, FS)),
        out_specs=(P(FS, TP), P(TP, FS), P(TP, FS), P(TP, FS), P(None, TP)),
        check_vma=False,
    )
```

time: 354 us -> 109 us (0.31)
  waiting for transfers between devices: 255 us -> 0 us
  Pallas kernels: 0 us -> 102 us
  matrix products: 38.5 us -> 0 us
  starting transfers between devices: 19.7 us -> 0 us
  between operations: 14.4 us -> 0.65 us
  other arithmetic: 13.6 us -> 1.49 us
  local copies, waits for them, and re-layouts: 11.4 us -> 5.46 us
    all_gather x2 -> x0, waiting for transfers between devices: 141 us -> none  [the longest x1 83.8 us: gather_turned(): whole = lax.all_gather(both, axis, axis=0, tiled=True)]
    pallas_call x0 -> x1, Pallas kernels: none -> 102 us  [on_device(): pl.pallas_call(kernel, out_shape=(jax.ShapeDtypeStruct((n, wide), BF16),...]
    unnamed x8 -> x0, waiting for transfers between devices: 47.5 us -> none
    dot_general x8 -> x0, matrix products: 38.5 us -> none  [the longest x6 29 us: contract(): lax.dot_general(left, right, (((left_dim,), (right_dim,)), ((), ())), pre...]
    reduce_scatter x2 -> x0, waiting for transfers between devices: 33.7 us -> none  [summed_rows(): nearer = lax.psum_scatter(x, axes[0], scatter_dimension=dim, tiled=True)]
    all_to_all x3 -> x0, waiting for transfers between devices: 32.3 us -> none  [the longest x2 26.4 us: sum_at_owner(): parts = lax.all_to_all(in_blocks(x, dim, peers), axis, 0, 0, tiled=True)]
    all_to_all x3 -> x0, starting transfers between devices: 19.3 us -> none  [the longest x2 10.8 us: sum_at_owner(): parts = lax.all_to_all(in_blocks(x, dim, peers), axis, 0, 0, tiled=True)]
    reduce_sum x6 -> x0, other arithmetic: 6.46 us -> none  [the longest x2 3.08 us: sum_at_owner(): return jnp.sum(parts.astype(jnp.float32), axis=0)]
  transfers between devices with their start and end apart: 9 -> 0, of which waited for: 7 -> 0; matrix products, arithmetic and copies ran while one was open for 13% -> 0% of each run, Pallas kernels for 0% -> 0%
where the time goes in v1:
time: 109 us
  Pallas kernels  102 us (94%)
  local copies, waits for them, and re-layouts  5.46 us (5%)
  other arithmetic  1.49 us (1%)
    pallas_call x1, Pallas kernels, on_device(): pl.pallas_call(kernel, out_shape=(jax.ShapeDtypeStruct((n, wide), BF16),...  102 us
    unnamed x6, local copies, waits for them, and re-layouts  3.23 us

profile of v1, /device:TPU:32, one launch (start us, length us, event | category | flops | bytes accessed | tf_op | source)
XLA Modules:
  0.0 109.2 jit_solution(18387076791444445623)
XLA Ops:
  0.6 1.5 %maximum_bitcast_fusion.wgu = bf16[64,768]{1,0:T(8,128)(2,1)} fusion(bf16[384,64]{0,1:T(8,128)(2,1)} %param.10, bf16[384,64]{0,1:T(8,128)(2,1)} %param.9), kind=kLoop, calls=%fused_computation | loop fusion | flops 196608 | bytes 196608 | tf_op jit(solution)/shard_map/transpose | solution.py:476
  2.1 101.6 %ffn_backward.1 = (bf16[1024,256]{1,0:T(8,128)(2,1)}, f32[64,768]{1,0:T(8,128)}, f32[64,384]{1,0:T(8,128)}, f32[1,1152]{1,0:T(1,128)}) custom-call(bf16[1024,256]{1,0:T(8,128)(2,1)} %tok.1, bf16[1024,256]{1,0:T(8,128)(2,1)} %grd.1, f32[8,1,256]{2,1,0:T(1,128)} %bitcast.11, bf16[64,768]{1,0:T(8,128)(2,1)} %maximum_bitcast_fusion.wgu, bf16[64,384]{1,0:T(8,128)(2,1)} %bitcast.10), custom_call_target="tpu_custom_call" | custom-call | tf_op jit(solution)/shard_map/ffn_backward/pallas_call | solution.py:516
  103.7 0.0 copy-start.1
  103.7 0.7 copy-done.1
  104.4 0.6 reshape.17
  105.0 1.6 %slice_bitcast_fusion = (f32[384,64]{0,1:T(8,128)}, f32[384,64]{0,1:T(8,128)}) fusion(f32[64,768]{1,0:T(8,128)} %get-tuple-element.10), kind=kLoop, calls=%fused_computation.1 | loop fusion | bytes 393216 | tf_op jit(solution)/shard_map/transpose | solution.py:540
  106.6 0.0 copy-start
  106.6 1.9 %copy.13 = bf16[1024,256]{1,0:T(8,128)(2,1)} copy(bf16[1024,256]{1,0:T(8,128)(2,1)} %get-tuple-element.20) | data formatting | bytes 1048576
  108.5 0.0 copy-done
  108.5 0.6 copy.14
  (1 shorter events, 0.0 us)
Async XLA Ops:
  103.7 0.7 copy-start.1
  106.6 1.9 %copy-start = (f32[64,384]{1,0:T(8,128)S(1)}, f32[64,384]{1,0:T(8,128)}, u32[]{:S(2)}) copy-start(f32[64,384]{1,0:T(8,128)} %get-tuple-element.11) | copy-start | bytes 294916

commit v2 on v1

--- a/solution.py
+++ b/solution.py
@@ -11,7 +11,8 @@
 NZ, NX, NY, NC = 8, 4, 4, 2
 F32, BF16 = jnp.float32, jnp.bfloat16
 CHUNKS = 4
-COPIES = 184
+COPIES = 196
+SPANS = ((0, 256), (256, 256), (512, 256), (768, 128), (896, 128))
 ORDER = (4, 3, -3, 2, -2, 1, -1, 0)
 
 
@@ -50,11 +51,11 @@
 
 
 def kernel(
-    tok, grd, gain, wgu, wdn,
-    out_in, out_gu, out_dn, out_sq,
+    tok, grd, gain, wg, wu, wd,
+    out_in, out_g, out_u, out_d, out_sq,
     T, G, N, GU, DN, AB, H, INV, V, DGU, DDN,
     SX1, RX1, SX2, RX2, XR, SZ, RZ, SD, RD, FD, SE1, RE1, SE2, RE2,
-    PP, PR, S1, R1, S2, R2, QX, QZ,
+    PP, PR, S1, R1, S2, R2, QX, QZ, IN, LG, LU, LD,
     send_sems, recv_sems, local_sems,
 ):
     z, x, y, c = (lax.axis_index(a) for a in ("z", "x", "y", "c"))
@@ -67,27 +68,33 @@
     tokens = tok.shape[0]
     rows = tokens // CHUNKS
     wide = tok.shape[1]
-    ff = wdn.shape[1]
+    part, ff = wd.shape
     model = wide * NY * NC
-    part = wgu.shape[0]
     half_part, half_rows = part // 2, rows // 2
     gate, up = pl.ds(0, ff), pl.ds(ff, ff)
     factor = (tokens * NZ * NX) ** (-0.5)
     span = lambda ch: pl.ds(ch * rows, rows)
+    some = lambda ch: pl.ds(*SPANS[ch])
 
     barrier = pltpu.get_barrier_semaphore()
-    peers = [{"z": zz(d)} for d in range(1, NZ)] + [{"x": xx(d)} for d in range(1, NX)]
-    peers += [{"y": yy(1)}, {"y": yy(-1)}, {"c": other}]
+    peers = [{a: p} for a, n in (("z", zz), ("x", xx), ("y", yy)) for p in (n(1), n(-1))]
+    peers += [{"c": other}]
     for peer in peers:
         pl.semaphore_signal(barrier, inc=1, device_id=peer, device_id_type=pl.DeviceIdType.MESH)
+    loads = (
+        (wg, GU.at[z, x, :, gate]),
+        (wu, GU.at[z, x, :, up]),
+        (wd, DN.at[z, x]),
+        (tok, T.at[me]),
+        (grd, G.at[me]),
+    )
     locals_ = [
-        pltpu.make_async_copy(src, dst, local_sems.at[i])
-        for i, (src, dst) in enumerate(
-            ((wgu, GU.at[z, x]), (wdn, DN.at[z, x]), (tok, T.at[me]), (grd, G.at[me]))
-        )
+        pltpu.make_async_copy(src, dst, local_sems.at[i]) for i, (src, dst) in enumerate(loads)
     ]
     for copy in locals_:
         copy.start()
+    for copy in locals_:
+        copy.wait()
     pl.semaphore_wait(barrier, len(peers))
     net = Net(send_sems, recv_sems)
 
@@ -141,20 +148,20 @@
 
     def y_own(ch):
         for way in (1, -1):
-            ya["T", ch, way] = net.send(tok.at[span(ch)], T.at[me, span(ch)], y=yy(way))
-            ya["G", ch, way] = net.send(grd.at[span(ch)], G.at[me, span(ch)], y=yy(way))
+            ya["T", ch, way] = net.send(T.at[me, some(ch)], T.at[me, some(ch)], y=yy(way))
+            ya["G", ch, way] = net.send(G.at[me, some(ch)], G.at[me, some(ch)], y=yy(way))
 
     def to_other(name, full, d, ch):
-        ref = full.at[slot(d), span(ch)]
+        ref = full.at[slot(d), some(ch)]
         dd[name, d, ch] = net.send(ref, ref, c=other)
 
     def y_pass(ch):
         ya["T", ch, 1].wait_recv()
-        ref = T.at[slot(-1), span(ch)]
+        ref = T.at[slot(-1), some(ch)]
         yb["T", ch] = net.send(ref, ref, y=yy(1))
         to_other("T", T, -1, ch)
         ya["G", ch, -1].wait_recv()
-        ref = G.at[slot(1), span(ch)]
+        ref = G.at[slot(1), some(ch)]
         yb["G", ch] = net.send(ref, ref, y=yy(-1))
         to_other("G", G, 1, ch)
         ya["G", ch, 1].wait_recv()
@@ -172,42 +179,43 @@
         if ch == 0:
             dd["T"].wait_recv()
             dd["G"].wait_recv()
-            locals_[2].wait()
-            locals_[3].wait()
         for d in (-1, 1, 2):
             dd["T", d, ch].wait_recv()
             dd["G", d, ch].wait_recv()
 
     def norm(ch):
-        total = jnp.zeros((rows, 128), F32)
+        total = jnp.zeros((SPANS[ch][1], 128), F32)
         for k in range(NY * NC):
-            t = T[k, span(ch)].astype(F32)
+            t = T[k, some(ch)].astype(F32)
             total = total + lanes_summed(t * t)
         inv = lax.rsqrt(jnp.sum(total, axis=1, keepdims=True) / model + 1e-06)
-        INV[span(ch)] = inv
+        INV[some(ch)] = inv
         for k in range(NY * NC):
-            t = T[k, span(ch)].astype(F32)
-            N[k, span(ch)] = (t * inv * gain[k]).astype(BF16)
+            t = T[k, some(ch)].astype(F32)
+            N[k, some(ch)] = (t * inv * gain[k]).astype(BF16)
 
     def forward(ch):
-        pre = jnp.zeros((rows, 2 * ff), F32)
-        gh = jnp.zeros((rows, ff), F32)
+        pre = jnp.zeros((SPANS[ch][1], 2 * ff), F32)
+        gh = jnp.zeros((SPANS[ch][1], ff), F32)
         for k in range(NY * NC):
             pre = pre + jnp.dot(
-                N[k, span(ch)], GU[k].reshape(wide, 2 * ff), preferred_element_type=F32
+                N[k, some(ch)], GU[k].reshape(wide, 2 * ff), preferred_element_type=F32
             )
-            gh = gh + jnp.dot(G[k, span(ch)], DN[k].reshape(wide, ff), preferred_element_type=F32)
+            gh = gh + jnp.dot(G[k, some(ch)], DN[k].reshape(wide, ff), preferred_element_type=F32)
         gh = 0.5 * gh
         g, u = pre[:, 0:ff], pre[:, ff : 2 * ff]
         sigma = jax.nn.sigmoid(g)
         active = g * sigma
-        H[span(ch)] = (active * u).astype(BF16)
-        AB[span(ch), 0:ff] = (gh * u * sigma * (1.0 + g * (1.0 - sigma))).astype(BF16)
-        AB[span(ch), ff : 2 * ff] = (gh * active).astype(BF16)
+        H[some(ch)] = (active * u).astype(BF16)
+        AB[some(ch), 0:ff] = (gh * u * sigma * (1.0 + g * (1.0 - sigma))).astype(BF16)
+        AB[some(ch), ff : 2 * ff] = (gh * active).astype(BF16)
 
     def weights(d):
         k = zz(d)
         DGU[k] = (factor * turned(N[k], AB[...])).reshape(NX, part, 2 * ff)
+
+    def downs(d):
+        k = zz(d)
         DDN[k] = (0.5 * factor * turned(G[k], H[...])).reshape(NX, part, ff)
 
     def partial(ch):
@@ -354,22 +362,72 @@
         ).astype(BF16)
         p2[ch, -1] = net.send(S2.at[ch, 1], R2.at[ch, 1], y=yy(-1))
 
+    stores = []
+
+    def store(src, dst):
+        copy = pltpu.make_async_copy(src, dst, local_sems.at[len(loads) + len(stores)])
+        copy.start()
+        stores.append(copy)
+
     def p_sum(ch):
         p2[ch, 1].wait_recv()
         p2[ch, -1].wait_recv()
         total = p_pair(ch, 0, 0, rows) + R2[ch, 0].astype(F32) + R2[ch, 1].astype(F32)
-        out_in[span(ch)] = (grd[span(ch)].astype(F32) + total).astype(BF16)
-
-    for way in (1, -1):
-        gz[1, way] = net.send(wgu, GU.at[z, x], z=zz(way))
-        dx[way] = net.send(wdn, DN.at[z, x], x=xx(way))
-    gx_send(0, wgu)
-    y_own(0)
-    dd["T"] = net.send(tok, T.at[me], c=other)
-    dd["G"] = net.send(grd, G.at[me], c=other)
-    y_own(1)
-    locals_[0].wait()
-    locals_[1].wait()
+        IN[span(ch)] = total
+        store(IN.at[span(ch)], out_in.at[span(ch)])
+
+    def begin():
+        for way in (1, -1):
+            gz[1, way] = net.send(GU.at[z, x], GU.at[z, x], z=zz(way))
+            dx[way] = net.send(DN.at[z, x], DN.at[z, x], x=xx(way))
+        gx_send(0, GU.at[z, x])
+        y_own(0)
+        dd["T"] = net.send(T.at[me], T.at[me], c=other)
+        dd["G"] = net.send(G.at[me], G.at[me], c=other)
+        y_own(1)
+
+    def e_finish():
+        down = e_sum()
+        LD[...] = down
+        store(LD, out_d)
+        QX[x, :, pl.ds(2 * ff, ff)] = jnp.sum(down * down, axis=0, keepdims=True)
+
+    def z_finish():
+        both = z_step(steps - 1)
+        LG[...] = both[:, 0:ff]
+        LU[...] = both[:, ff : 2 * ff]
+        store(LG, out_g)
+        store(LU, out_u)
+        QX[x, :, pl.ds(0, 2 * ff)] = jnp.sum(both * both, axis=0, keepdims=True)
+
+    def q_x():
+        sent = [net.send(QX.at[x], QX.at[x], x=xx(d)) for d in (2, 1, 3)]
+        for copy in sent:
+            copy.wait_recv()
+        total = QX[0]
+        for at in range(1, NX):
+            total = total + QX[at]
+        QZ[z] = total
+
+    def q_z():
+        sent = [net.send(QZ.at[z], QZ.at[z], z=zz(d)) for d in (4, 3, 5, 2, 6, 1, 7)]
+        for copy in sent:
+            copy.wait_recv()
+        total = QZ[0]
+        for at in range(1, NZ):
+            total = total + QZ[at]
+        total = total / model
+        for at in range(3):
+            out_sq[pl.ds(at, 1)] = total[:, at * ff : (at + 1) * ff]
+
+    def finish():
+        assert len(net.copies) == COPIES, len(net.copies)
+        net.finish()
+        for copy in stores:
+            copy.wait()
+
+    steps = len(ORDER)
+    begin()
     dx_pass()
     gz_step(1)
     gx_pass(0)
@@ -384,6 +442,7 @@
     dz_step(1)
     y_pass(1)
     y_own(3)
+    y_own(4)
     gz_step(3)
     gx_pass(-2)
     gx_pass(2)
@@ -406,6 +465,7 @@
         gxf[d, 1].wait_recv()
         gxf[d, -1].wait_recv()
     forward(0)
+    y_pass(4)
     y_last(2)
     y_ready(2)
     norm(2)
@@ -414,58 +474,51 @@
     y_ready(3)
     norm(3)
     forward(2)
+    y_last(4)
     forward(3)
-
-    steps = len(ORDER)
+    y_ready(4)
+    norm(4)
+    forward(4)
+
+    downs(ORDER[0])
+    d_step(0)
     for i in range(steps):
+        if i in (3, 5):
+            d_step(i)
+            d_step(i + 1)
+        if i == 7:
+            d_step(i)
+            e_step1()
         weights(ORDER[i])
         x_step1(i)
-        d_step(i)
         if i >= 1:
             x_step2(i - 1)
-        if i % 2 == 0:
-            partial(i // 2)
-            p_send(i // 2)
-        else:
-            p_step1(i // 2)
-            if i >= 3:
-                p_step2(i // 2 - 1)
+        if i < CHUNKS:
+            partial(i)
+            p_send(i)
+        if i == 1:
+            d_step(1)
+            d_step(2)
+        for j in (2 * i + 1, 2 * i + 2):
+            if j < steps:
+                downs(ORDER[j])
+        if 1 <= i <= CHUNKS:
+            p_step1(i - 1)
+        if 3 <= i < CHUNKS + 3:
+            p_step2(i - 3)
+        if i >= 5:
+            p_sum(i - 5)
         if i >= 2:
             z_step(i - 2)
     x_step2(steps - 1)
-    e_step1()
-    p_step2(CHUNKS - 1)
     z_step(steps - 2)
     e_step2()
-    for ch in range(CHUNKS - 1):
-        p_sum(ch)
-    down = e_sum()
-    out_dn[...] = down
-    both = z_step(steps - 1)
-    out_gu[...] = both
     p_sum(CHUNKS - 1)
-
-    squares = jnp.concatenate(
-        [jnp.sum(both * both, axis=0, keepdims=True), jnp.sum(down * down, axis=0, keepdims=True)],
-        axis=1,
-    )
-    QX[x] = squares
-    sent = [net.send(QX.at[x], QX.at[x], x=xx(d)) for d in range(1, NX)]
-    for copy in sent:
-        copy.wait_recv()
-    total = QX[0]
-    for at in range(1, NX):
-        total = total + QX[at]
-    QZ[z] = total
-    sent = [net.send(QZ.at[z], QZ.at[z], z=zz(d)) for d in range(1, NZ)]
-    for copy in sent:
-        copy.wait_recv()
-    total = QZ[0]
-    for at in range(1, NZ):
-        total = total + QZ[at]
-    out_sq[...] = total / model
-    assert len(net.copies) == COPIES, len(net.copies)
-    net.finish()
+    z_finish()
+    e_finish()
+    q_x()
+    q_z()
+    finish()
 
 
 def on_device(tokens, grad_out, norm_gain, gate_weight, up_weight, down_weight):
@@ -473,10 +526,9 @@
     ff, part = gate_weight.shape
     blocks = NY * NC
     rows = n // CHUNKS
-    wgu = jnp.concatenate([gate_weight, up_weight], axis=0).T
-    wdn = down_weight.T
     gain = norm_gain.reshape(blocks, 1, wide)
     vm = pl.BlockSpec(memory_space=pltpu.VMEM)
+    hbm = pl.BlockSpec(memory_space=pl.ANY)
     half = NZ // 2
     scratch = [
         ((blocks, n, wide), BF16),
@@ -512,35 +564,36 @@
         ((CHUNKS, 2, rows, wide), BF16),
         ((NX, 1, 3 * ff), F32),
         ((NZ, 1, 3 * ff), F32),
+        ((n, wide), F32),
+        ((part, ff), F32),
+        ((part, ff), F32),
+        ((part, ff), F32),
     ]
-    grad_in, grad_gu, grad_dn, squares = pl.pallas_call(
+    grad = jax.ShapeDtypeStruct((part, ff), F32)
+    total, grad_gate, grad_up, grad_down, squares = pl.pallas_call(
         kernel,
         out_shape=(
-            jax.ShapeDtypeStruct((n, wide), BF16),
-            jax.ShapeDtypeStruct((part, 2 * ff), F32),
-            jax.ShapeDtypeStruct((part, ff), F32),
-            jax.ShapeDtypeStruct((1, 3 * ff), F32),
+            jax.ShapeDtypeStruct((n, wide), F32),
+            grad,
+            grad,
+            grad,
+            jax.ShapeDtypeStruct((3, ff), F32),
         ),
-        in_specs=[vm] * 5,
-        out_specs=(vm,) * 4,
+        in_specs=[hbm, hbm, vm, hbm, hbm, hbm],
+        out_specs=(hbm, hbm, hbm, hbm, vm),
         scratch_shapes=[pltpu.VMEM(shape, dtype) for shape, dtype in scratch]
         + [
             pltpu.SemaphoreType.DMA((COPIES,)),
             pltpu.SemaphoreType.DMA((COPIES,)),
-            pltpu.SemaphoreType.DMA((4,)),
+            pltpu.SemaphoreType.DMA((12,)),
         ],
         compiler_params=pltpu.CompilerParams(
             collective_id=0, has_side_effects=True, vmem_limit_bytes=67043328
         ),
         name="ffn_backward",
-    )(tokens, grad_out, gain, wgu, wdn)
-    return (
-        grad_in,
-        grad_gu[:, :ff].T,
-        grad_gu[:, ff:].T,
-        grad_dn.T,
-        squares.reshape(3, ff),
-    )
+    )(tokens, grad_out, gain, gate_weight.T, up_weight.T, down_weight.T)
+    grad_in = (grad_out.astype(F32) + total).astype(BF16)
+    return grad_in, grad_gate.T, grad_up.T, grad_down.T, squares
 
 
 def solution(mesh):

time: 109 us -> 107 us (0.982)
  local copies, waits for them, and re-layouts: 5.46 us -> 3.14 us
    convert_element_type x0 -> x1, other arithmetic: none -> 2.3 us  [on_device(): grad_in = (grad_out.astype(F32) + total).astype(BF16)]
    transpose x1 -> x0, local copies, waits for them, and re-layouts: 1.63 us -> none  [on_device(): grad_gu[:, ff:]]
    transpose x1 -> x0, other arithmetic: 1.47 us -> none  [on_device(): wgu = jnp.concatenate([gate_weight, up_weight], axis=0).T]
    unnamed x6 -> x12, local copies, waits for them, and re-layouts: 3.23 us -> 3.14 us
where the time goes in v2:
time: 107 us
  Pallas kernels  101 us (94%)
  local copies, waits for them, and re-layouts  3.14 us (3%)
  other arithmetic  2.3 us (2%)
    pallas_call x1, Pallas kernels, on_device(): pl.pallas_call(kernel, out_shape=(jax.ShapeDtypeStruct((n, wide), F32), g...  101 us
    unnamed x12, local copies, waits for them, and re-layouts  3.14 us
    convert_element_type x1, other arithmetic, on_device(): grad_in = (grad_out.astype(F32) + total).astype(BF16)  2.3 us

profile of v2, /device:TPU:32, one launch (start us, length us, event | category | flops | bytes accessed | tf_op | source)
XLA Modules:
  0.0 107.0 jit_solution(16398180229809567634)
XLA Ops:
  0.6 100.9 %ffn_backward.1 = (f32[1024,256]{1,0:T(8,128)}, f32[64,384]{1,0:T(8,128)}, f32[64,384]{1,0:T(8,128)}, f32[64,384]{1,0:T(8,128)}, f32[3,384]{1,0:T(4,128)}) custom-call(bf16[1024,256]{1,0:T(8,128)(2,1)} %tok.1, bf16[1024,256]{1,0:T(8,128)(2,1)} %grd.1, f32[8,1,256]{2,1,0:T(1,128)} %bitcast.13, bf16[64,384]{1,0:T(8,128)(2,1)} %bitcast.10, ...), custom_call_target="tpu_custom_call" | custom-call | tf_op jit(solution)/shard_map/ffn_backward/pallas_call | solution.py:573
  101.6 0.0 copy-start.2
  101.6 2.3 %add_convert_fusion = bf16[1024,256]{1,0:T(8,128)(2,1)} fusion(f32[1024,256]{1,0:T(8,128)} %get-tuple-element.10, bf16[1024,256]{1,0:T(8,128)(2,1)} %grd.1), kind=kLoop, calls=%fused_computation | loop fusion | flops 786432 | bytes 2097152 | tf_op jit(solution)/shard_map/convert_element_type | solution.py:595
  103.9 0.0 copy-done.2
  103.9 0.0 copy-start.1
  103.9 0.6 copy.15
  104.5 0.3 copy-done.1
  104.8 0.0 copy-start
  104.8 0.6 copy.16
  105.4 0.3 copy-done
  105.7 0.0 copy-start.3
  105.7 0.6 copy.17
  106.4 0.0 copy-done.3
  106.4 0.6 copy.18
Async XLA Ops:
  101.6 2.3 %copy-start.2 = (f32[64,384]{1,0:T(8,128)S(1)}, f32[64,384]{1,0:T(8,128)}, u32[]{:S(2)}) copy-start(f32[64,384]{1,0:T(8,128)} %get-tuple-element.11) | copy-start | bytes 294916
  103.9 0.9 copy-start.1
  104.8 0.9 copy-start
  105.7 0.7 copy-start.3

commit v3 on v2

--- a/solution.py
+++ b/solution.py
@@ -11,7 +11,8 @@
 NZ, NX, NY, NC = 8, 4, 4, 2
 F32, BF16 = jnp.float32, jnp.bfloat16
 CHUNKS = 4
-COPIES = 196
+ARRIVALS = 139
+TURNS = 56
 SPANS = ((0, 256), (256, 256), (512, 256), (768, 128), (896, 128))
 ORDER = (4, 3, -3, 2, -2, 1, -1, 0)
 
@@ -19,14 +20,22 @@
 class Net:
     def __init__(self, send_sems, recv_sems):
         self.send_sems, self.recv_sems, self.copies = send_sems, recv_sems, []
-
-    def send(self, src, dst, **to):
+        self.groups, self.used = {}, 0
+
+    def send(self, src, dst, group=None, **to):
         at = len(self.copies)
+        if at >= TURNS:
+            self.copies[at - TURNS].wait_send()
+        if group is None:
+            group = ("one", at)
+        if group not in self.groups:
+            self.groups[group] = self.used
+            self.used += 1
         copy = pltpu.make_async_remote_copy(
             src_ref=src,
             dst_ref=dst,
-            send_sem=self.send_sems.at[at],
-            recv_sem=self.recv_sems.at[at],
+            send_sem=self.send_sems.at[at % TURNS],
+            recv_sem=self.recv_sems.at[self.groups[group]],
             device_id=to,
             device_id_type=pl.DeviceIdType.MESH,
         )
@@ -34,8 +43,11 @@
         self.copies.append(copy)
         return copy
 
+    def arrived(self, group, size):
+        pltpu.make_async_copy(size, size, self.recv_sems.at[self.groups[group]]).wait()
+
     def finish(self):
-        for copy in self.copies:
+        for copy in self.copies[-TURNS:]:
             copy.wait_send()
 
 
@@ -55,7 +67,7 @@
     out_in, out_g, out_u, out_d, out_sq,
     T, G, N, GU, DN, AB, H, INV, V, DGU, DDN,
     SX1, RX1, SX2, RX2, XR, SZ, RZ, SD, RD, FD, SE1, RE1, SE2, RE2,
-    PP, PR, S1, R1, S2, R2, QX, QZ, IN, LG, LU, LD,
+    PP, PR, S1, R1, S2, R2, QX, QZ, IN, LG, LU, LD, SQ,
     send_sems, recv_sems, local_sems,
 ):
     z, x, y, c = (lax.axis_index(a) for a in ("z", "x", "y", "c"))
@@ -81,24 +93,25 @@
     peers += [{"c": other}]
     for peer in peers:
         pl.semaphore_signal(barrier, inc=1, device_id=peer, device_id_type=pl.DeviceIdType.MESH)
+    head, rest = some(0), pl.ds(SPANS[0][1], tokens - SPANS[0][1])
     loads = (
+        (tok.at[head], T.at[me, head]),
+        (grd.at[head], G.at[me, head]),
+        (wd, DN.at[z, x]),
         (wg, GU.at[z, x, :, gate]),
         (wu, GU.at[z, x, :, up]),
-        (wd, DN.at[z, x]),
-        (tok, T.at[me]),
-        (grd, G.at[me]),
+        (tok.at[rest], T.at[me, rest]),
+        (grd.at[rest], G.at[me, rest]),
     )
     locals_ = [
         pltpu.make_async_copy(src, dst, local_sems.at[i]) for i, (src, dst) in enumerate(loads)
     ]
     for copy in locals_:
         copy.start()
-    for copy in locals_:
-        copy.wait()
     pl.semaphore_wait(barrier, len(peers))
     net = Net(send_sems, recv_sems)
 
-    gz, gx, gxf, dx, dxf, dz, ya, yb, dd = {}, {}, {}, {}, {}, {}, {}, {}, {}
+    gz, gx, dx, dz, ya, yb = {}, {}, {}, {}, {}, {}
 
     def gx_send(d, src):
         gx[d, 1] = net.send(src, GU.at[zz(d), x], x=xx(1))
@@ -107,10 +120,10 @@
     def gx_pass(d):
         gx[d, 1].wait_recv()
         ref = GU.at[zz(d), xx(-1), :, gate]
-        gxf[d, 1] = net.send(ref, ref, x=xx(1))
+        net.send(ref, ref, "gxf", x=xx(1))
         gx[d, -1].wait_recv()
         ref = GU.at[zz(d), xx(1), :, up]
-        gxf[d, -1] = net.send(ref, ref, x=xx(-1))
+        net.send(ref, ref, "gxf", x=xx(-1))
 
     def gz_step(s):
         for way in (1, -1):
@@ -129,22 +142,21 @@
     def dx_pass():
         dx[1].wait_recv()
         ref = DN.at[z, xx(-1), pl.ds(0, half_part)]
-        dxf[1] = net.send(ref, ref, x=xx(1))
+        net.send(ref, ref, "dxf", x=xx(1))
         dx[-1].wait_recv()
         ref = DN.at[z, xx(1), pl.ds(half_part, half_part)]
-        dxf[-1] = net.send(ref, ref, x=xx(-1))
-
-    def dz_step(s):
-        for way in (1, -1):
-            if s == 0:
-                ref = DN.at[z]
-            else:
-                dz[s, way].wait_recv()
-                ref = DN.at[zz(-way * s)]
-                if s == NZ // 2 - 1:
-                    ref = DN.at[zz(-way * s), pl.ds(0 if way == 1 else NX // 2, NX // 2)]
-            if s < NZ // 2:
-                dz[s + 1, way] = net.send(ref, ref, z=zz(way))
+        net.send(ref, ref, "dxf", x=xx(-1))
+
+    def dz_step(s, *pieces):
+        for dx_ in pieces:
+            for way in (1, -1):
+                if s > 0:
+                    dz[s, dx_, way].wait_recv()
+                ref = DN.at[zz(-way * s), xx(dx_)]
+                if s < NZ // 2 - 1:
+                    dz[s + 1, dx_, way] = net.send(ref, ref, z=zz(way))
+                elif (dx_ in (0, -1)) == (way == 1):
+                    net.send(ref, ref, "dz", z=zz(way))
 
     def y_own(ch):
         for way in (1, -1):
@@ -153,7 +165,7 @@
 
     def to_other(name, full, d, ch):
         ref = full.at[slot(d), some(ch)]
-        dd[name, d, ch] = net.send(ref, ref, c=other)
+        net.send(ref, ref, ("c", ch), c=other)
 
     def y_pass(ch):
         ya["T", ch, 1].wait_recv()
@@ -176,12 +188,9 @@
         to_other("G", G, 2, ch)
 
     def y_ready(ch):
-        if ch == 0:
-            dd["T"].wait_recv()
-            dd["G"].wait_recv()
-        for d in (-1, 1, 2):
-            dd["T", d, ch].wait_recv()
-            dd["G", d, ch].wait_recv()
+        of_all = 6 * SPANS[ch][1] + (2 * tokens if ch == 0 else 0)
+        lots = NY if ch == 0 else 3
+        net.arrived(("c", ch), PP.at[0, pl.ds(0, lots), pl.ds(0, of_all // lots)])
 
     def norm(ch):
         total = jnp.zeros((SPANS[ch][1], 128), F32)
@@ -236,29 +245,27 @@
             unit = T[k, span(ch)].astype(F32) * inv
             PP[k % NC, k // NC, span(ch)] = (inv * (V[k] - unit * inner)).astype(BF16)
 
-    x1, x2, zs, ds, e1, e2, pc, p1, p2 = {}, {}, {}, {}, {}, {}, {}, {}, {}
+    zs, ds, pc = {}, {}, {}
 
     def x_step1(i):
         k = zz(ORDER[i])
         SX1[i, 0] = DGU[k, xx(2), :, gate].astype(BF16)
         SX1[i, 1] = DGU[k, xx(2), :, up].astype(BF16)
-        x1[i, 1] = net.send(SX1.at[i, 0], RX1.at[i, 0], x=xx(1))
-        x1[i, -1] = net.send(SX1.at[i, 1], RX1.at[i, 1], x=xx(-1))
+        net.send(SX1.at[i, 0], RX1.at[i, 0], ("x1", i), x=xx(1))
+        net.send(SX1.at[i, 1], RX1.at[i, 1], ("x1", i), x=xx(-1))
 
     def x_step2(i):
         k = zz(ORDER[i])
-        x1[i, 1].wait_recv()
+        net.arrived(("x1", i), SX1.at[i])
         SX2[i, 0, :, gate] = (DGU[k, xx(1), :, gate] + RX1[i, 0].astype(F32)).astype(BF16)
         SX2[i, 0, :, up] = DGU[k, xx(1), :, up].astype(BF16)
-        x2[i, 1] = net.send(SX2.at[i, 0], RX2.at[i, 0], x=xx(1))
-        x1[i, -1].wait_recv()
+        net.send(SX2.at[i, 0], RX2.at[i, 0], ("x2", i), x=xx(1))
         SX2[i, 1, :, gate] = DGU[k, xx(-1), :, gate].astype(BF16)
         SX2[i, 1, :, up] = (DGU[k, xx(-1), :, up] + RX1[i, 1].astype(F32)).astype(BF16)
-        x2[i, -1] = net.send(SX2.at[i, 1], RX2.at[i, 1], x=xx(-1))
+        net.send(SX2.at[i, 1], RX2.at[i, 1], ("x2", i), x=xx(-1))
 
     def x_sum(i):
-        x2[i, 1].wait_recv()
-        x2[i, -1].wait_recv()
+        net.arrived(("x2", i), SX2.at[i])
         return DGU[zz(ORDER[i]), x] + RX2[i, 0].astype(F32) + RX2[i, 1].astype(F32)
 
     def z_step(i):
@@ -285,54 +292,48 @@
                 zs[way, abs(d)] = net.send(SZ.at[s, w], RZ.at[s, w], z=zz(way))
         return value
 
-    def d_step(i):
-        d = ORDER[i]
-        k = zz(d)
-        near = NX // 2
-        if d == NZ // 2:
-            SD[0, 0] = DDN[k].astype(BF16)
-            lo, hi = pl.ds(0, near), pl.ds(near, near)
-            ds[1, d] = net.send(SD.at[0, 0, lo], RD.at[0, 0, lo], z=zz(1))
-            ds[-1, d] = net.send(SD.at[0, 0, hi], RD.at[0, 1, hi], z=zz(-1))
-            return
-        if d == 0:
-            ds[1, 1].wait_recv()
-            ds[-1, 1].wait_recv()
-            last = NZ // 2 - 1
-            FD[...] = DDN[k] + RD[last, 0].astype(F32) + RD[last, 1].astype(F32)
-            return
-        way = 1 if d > 0 else -1
-        s, w = NZ // 2 - abs(d), 0 if way == 1 else 1
-        ds[way, abs(d) + 1].wait_recv()
-        if s == 1:
-            own = pl.ds(near if way == 1 else 0, near)
-            sent = pl.ds(0 if way == 1 else near, near)
-            SD[s, w, own] = DDN[k, own].astype(BF16)
-            SD[s, w, sent] = (DDN[k, sent] + RD[0, w, sent].astype(F32)).astype(BF16)
-        else:
-            SD[s, w] = (DDN[k] + RD[s - 1, w].astype(F32)).astype(BF16)
-        ds[way, abs(d)] = net.send(SD.at[s, w], RD.at[s, w], z=zz(way))
+    def d_step(d, way, half):
+        k, w = zz(d), 0 if way == 1 else 1
+        first = half == w
+        blocks = pl.ds(half * (NX // 2), NX // 2)
+        s = NZ // 2 - abs(d)
+        value = DDN[k, blocks]
+        if s >= (1 if first else 2):
+            ds[way, half, abs(d) + 1].wait_recv()
+            value = value + RD[s - 1, w, blocks].astype(F32)
+        SD[s, w, blocks] = value.astype(BF16)
+        group = "ds" if abs(d) == 1 else None
+        ds[way, half, abs(d)] = net.send(
+            SD.at[s, w, blocks], RD.at[s, w, blocks], group, z=zz(way)
+        )
+
+    def d_both(s, old):
+        for way in (1, -1):
+            d_step(way * (NZ // 2 - s), way, (0 if way == 1 else 1) if old else (1 if way == 1 else 0))
+
+    def d_sum():
+        last = NZ // 2 - 1
+        net.arrived("ds", SD.at[last])
+        FD[...] = DDN[z] + RD[last, 0].astype(F32) + RD[last, 1].astype(F32)
 
     def e_step1():
         SE1[...] = FD[xx(2)].astype(BF16)
         lo, hi = pl.ds(0, half_part), pl.ds(half_part, half_part)
-        e1[1] = net.send(SE1.at[lo], RE1.at[lo], x=xx(1))
-        e1[-1] = net.send(SE1.at[hi], RE1.at[hi], x=xx(-1))
+        net.send(SE1.at[lo], RE1.at[lo], "e1", x=xx(1))
+        net.send(SE1.at[hi], RE1.at[hi], "e1", x=xx(-1))
 
     def e_step2():
         lo, hi = pl.ds(0, half_part), pl.ds(half_part, half_part)
-        e1[1].wait_recv()
+        net.arrived("e1", SE1)
         SE2[0, lo] = (FD[xx(1), lo] + RE1[lo].astype(F32)).astype(BF16)
         SE2[0, hi] = FD[xx(1), hi].astype(BF16)
-        e2[1] = net.send(SE2.at[0], RE2.at[0], x=xx(1))
-        e1[-1].wait_recv()
+        net.send(SE2.at[0], RE2.at[0], "e2", x=xx(1))
         SE2[1, lo] = FD[xx(-1), lo].astype(BF16)
         SE2[1, hi] = (FD[xx(-1), hi] + RE1[hi].astype(F32)).astype(BF16)
-        e2[-1] = net.send(SE2.at[1], RE2.at[1], x=xx(-1))
+        net.send(SE2.at[1], RE2.at[1], "e2", x=xx(-1))
 
     def e_sum():
-        e2[1].wait_recv()
-        e2[-1].wait_recv()
+        net.arrived("e2", SE2)
         return FD[x] + RE2[0].astype(F32) + RE2[1].astype(F32)
 
     def p_send(ch):
@@ -346,21 +347,20 @@
         pc[ch].wait_recv()
         S1[ch] = p_pair(ch, 2, 0, rows).astype(BF16)
         lo, hi = pl.ds(0, half_rows), pl.ds(half_rows, half_rows)
-        p1[ch, 1] = net.send(S1.at[ch, lo], R1.at[ch, lo], y=yy(1))
-        p1[ch, -1] = net.send(S1.at[ch, hi], R1.at[ch, hi], y=yy(-1))
+        net.send(S1.at[ch, lo], R1.at[ch, lo], ("p1", ch), y=yy(1))
+        net.send(S1.at[ch, hi], R1.at[ch, hi], ("p1", ch), y=yy(-1))
 
     def p_step2(ch):
         lo, hi = pl.ds(0, half_rows), pl.ds(half_rows, half_rows)
-        p1[ch, 1].wait_recv()
+        net.arrived(("p1", ch), S1.at[ch])
         S2[ch, 0, lo] = (p_pair(ch, 1, 0, half_rows) + R1[ch, lo].astype(F32)).astype(BF16)
         S2[ch, 0, hi] = p_pair(ch, 1, half_rows, half_rows).astype(BF16)
-        p2[ch, 1] = net.send(S2.at[ch, 0], R2.at[ch, 0], y=yy(1))
-        p1[ch, -1].wait_recv()
+        net.send(S2.at[ch, 0], R2.at[ch, 0], ("p2", ch), y=yy(1))
         S2[ch, 1, lo] = p_pair(ch, -1, 0, half_rows).astype(BF16)
         S2[ch, 1, hi] = (
             p_pair(ch, -1, half_rows, half_rows) + R1[ch, hi].astype(F32)
         ).astype(BF16)
-        p2[ch, -1] = net.send(S2.at[ch, 1], R2.at[ch, 1], y=yy(-1))
+        net.send(S2.at[ch, 1], R2.at[ch, 1], ("p2", ch), y=yy(-1))
 
     stores = []
 
@@ -370,21 +370,27 @@
         stores.append(copy)
 
     def p_sum(ch):
-        p2[ch, 1].wait_recv()
-        p2[ch, -1].wait_recv()
+        net.arrived(("p2", ch), S2.at[ch])
         total = p_pair(ch, 0, 0, rows) + R2[ch, 0].astype(F32) + R2[ch, 1].astype(F32)
-        IN[span(ch)] = total
+        IN[span(ch)] = (G[me, span(ch)].astype(F32) + total).astype(BF16)
         store(IN.at[span(ch)], out_in.at[span(ch)])
 
     def begin():
+        locals_[0].wait()
+        locals_[1].wait()
+        y_own(0)
+        for copy in locals_[2:5]:
+            copy.wait()
         for way in (1, -1):
             gz[1, way] = net.send(GU.at[z, x], GU.at[z, x], z=zz(way))
             dx[way] = net.send(DN.at[z, x], DN.at[z, x], x=xx(way))
+        dz_step(0, 0)
         gx_send(0, GU.at[z, x])
-        y_own(0)
-        dd["T"] = net.send(T.at[me], T.at[me], c=other)
-        dd["G"] = net.send(G.at[me], G.at[me], c=other)
+        for copy in locals_[5:]:
+            copy.wait()
         y_own(1)
+        net.send(T.at[me], T.at[me], ("c", 0), c=other)
+        net.send(G.at[me], G.at[me], ("c", 0), c=other)
 
     def e_finish():
         down = e_sum()
@@ -401,27 +407,30 @@
         QX[x, :, pl.ds(0, 2 * ff)] = jnp.sum(both * both, axis=0, keepdims=True)
 
     def q_x():
-        sent = [net.send(QX.at[x], QX.at[x], x=xx(d)) for d in (2, 1, 3)]
-        for copy in sent:
-            copy.wait_recv()
+        for d in (2, 1, 3):
+            net.send(QX.at[x], QX.at[x], "qx", x=xx(d))
+        p_sum(2)
+        net.arrived("qx", QX.at[pl.ds(0, NX - 1)])
         total = QX[0]
         for at in range(1, NX):
             total = total + QX[at]
         QZ[z] = total
 
     def q_z():
-        sent = [net.send(QZ.at[z], QZ.at[z], z=zz(d)) for d in (4, 3, 5, 2, 6, 1, 7)]
-        for copy in sent:
-            copy.wait_recv()
+        for d in (4, 3, 5, 2, 6, 1, 7):
+            net.send(QZ.at[z], QZ.at[z], "qz", z=zz(d))
+        p_sum(3)
+        net.arrived("qz", QZ.at[pl.ds(0, NZ - 1)])
         total = QZ[0]
         for at in range(1, NZ):
             total = total + QZ[at]
         total = total / model
         for at in range(3):
-            out_sq[pl.ds(at, 1)] = total[:, at * ff : (at + 1) * ff]
+            SQ[pl.ds(at, 1)] = total[:, at * ff : (at + 1) * ff]
+        store(SQ, out_sq)
 
     def finish():
-        assert len(net.copies) == COPIES, len(net.copies)
+        assert net.used == ARRIVALS, net.used
         net.finish()
         for copy in stores:
             copy.wait()
@@ -430,95 +439,143 @@
     begin()
     dx_pass()
     gz_step(1)
+    dz_step(0, -1, 1)
     gx_pass(0)
-    dxf[1].wait_recv()
-    dxf[-1].wait_recv()
-    dz_step(0)
+    dz_step(1, 0)
+    net.arrived("dxf", DN.at[0, 0])
     y_pass(0)
     y_own(2)
     gz_step(2)
+    dz_step(0, 2)
     gx_pass(-1)
+    dz_step(1, -1, 1)
     gx_pass(1)
-    dz_step(1)
     y_pass(1)
     y_own(3)
     y_own(4)
     gz_step(3)
+    dz_step(2, 0)
+    dz_step(1, 2)
+    y_last(0)
     gx_pass(-2)
+    gz_step(4)
     gx_pass(2)
-    dz_step(2)
-    y_last(0)
-    y_ready(0)
-    norm(0)
-    gz_step(4)
+    dz_step(2, -1, 1)
+    dz_step(3, 0)
+    dz_step(2, 2)
     y_pass(2)
     gx_pass(-3)
     gx_pass(3)
-    dz_step(3)
+    dz_step(3, -1, 1)
     y_last(1)
+    dz_step(3, 2)
+    y_ready(0)
+    norm(0)
+    gx_pass(4)
+    y_pass(3)
+    net.arrived("dz", DN.at[0])
+    net.arrived("gxf", DN.at[pl.ds(0, 4)])
+    forward(0)
     y_ready(1)
     norm(1)
-    gx_pass(4)
-    y_pass(3)
-    dz_step(4)
-    for d in (0, -1, 1, -2, 2, -3, 3, 4):
-        gxf[d, 1].wait_recv()
-        gxf[d, -1].wait_recv()
-    forward(0)
     y_pass(4)
+    forward(1)
     y_last(2)
     y_ready(2)
     norm(2)
-    forward(1)
     y_last(3)
+    forward(2)
+    y_last(4)
     y_ready(3)
     norm(3)
-    forward(2)
-    y_last(4)
     forward(3)
     y_ready(4)
     norm(4)
     forward(4)
 
+    ahead = 3
+    weights(ORDER[0])
+    x_step1(0)
     downs(ORDER[0])
-    d_step(0)
-    for i in range(steps):
-        if i in (3, 5):
-            d_step(i)
-            d_step(i + 1)
-        if i == 7:
-            d_step(i)
-            e_step1()
-        weights(ORDER[i])
-        x_step1(i)
-        if i >= 1:
-            x_step2(i - 1)
+    d_both(0, True)
+    weights(ORDER[1])
+    x_step1(1)
+    downs(ORDER[1])
+    downs(ORDER[2])
+    d_both(1, False)
+    weights(ORDER[2])
+    x_step1(2)
+    for i in range(5):
+        x_step2(i)
+        weights(ORDER[i + ahead])
+        x_step1(i + ahead)
+        if i == 0:
+            downs(ORDER[3])
+            downs(ORDER[4])
+            d_both(1, True)
+        if i == 1:
+            d_both(2, False)
+        if i == 2:
+            downs(ORDER[5])
+            downs(ORDER[6])
+            d_both(2, True)
+        if i == 3:
+            d_both(3, False)
+        if i == 4:
+            downs(ORDER[7])
+            d_both(3, True)
+        if i >= 2:
+            p_step1(i - 2)
         if i < CHUNKS:
             partial(i)
             p_send(i)
-        if i == 1:
-            d_step(1)
-            d_step(2)
-        for j in (2 * i + 1, 2 * i + 2):
-            if j < steps:
-                downs(ORDER[j])
-        if 1 <= i <= CHUNKS:
-            p_step1(i - 1)
-        if 3 <= i < CHUNKS + 3:
-            p_step2(i - 3)
-        if i >= 5:
-            p_sum(i - 5)
-        if i >= 2:
-            z_step(i - 2)
-    x_step2(steps - 1)
-    z_step(steps - 2)
+        if i >= 1:
+            z_step(i - 1)
+    x_step2(5)
+    p_step1(3)
+    p_step2(0)
+    x_step2(6)
+    z_step(4)
+    x_step2(7)
+    p_step2(1)
+    d_sum()
+    e_step1()
+    z_step(5)
+    p_step2(2)
+    z_step(6)
     e_step2()
-    p_sum(CHUNKS - 1)
+    p_step2(3)
+    p_sum(0)
+    p_sum(1)
     z_finish()
     e_finish()
     q_x()
     q_z()
     finish()
+
+
+def deliver(*refs):
+    n = (len(refs) - 2) // 3
+    given, taken, held = refs[:n], refs[n : 2 * n], refs[2 * n : 3 * n]
+    in_sems, out_sems = refs[3 * n :]
+    parts = []
+    for src, mid, dst in zip(given, held, taken):
+        step = min(src.shape[0], 256)
+        for at in range(0, src.shape[0], step):
+            sub, i = pl.ds(at, step), len(parts)
+            parts.append(
+                (
+                    pltpu.make_async_copy(src.at[sub], mid.at[sub], in_sems.at[i]),
+                    pltpu.make_async_copy(mid.at[sub], dst.at[sub], out_sems.at[i]),
+                )
+            )
+    for load, _ in parts:
+        load.start()
+    for load, save in parts:
+        load.wait()
+        save.start()
+    for _, save in parts:
+        save.wait()
 
 
 def on_device(tokens, grad_out, norm_gain, gate_weight, up_weight, down_weight):
@@ -564,35 +621,46 @@
         ((CHUNKS, 2, rows, wide), BF16),
         ((NX, 1, 3 * ff), F32),
         ((NZ, 1, 3 * ff), F32),
-        ((n, wide), F32),
+        ((n, wide), BF16),
         ((part, ff), F32),
         ((part, ff), F32),
         ((part, ff), F32),
+        ((3, ff), F32),
     ]
     grad = jax.ShapeDtypeStruct((part, ff), F32)
-    total, grad_gate, grad_up, grad_down, squares = pl.pallas_call(
+    grad_in, grad_gate, grad_up, grad_down, squares = pl.pallas_call(
         kernel,
         out_shape=(
-            jax.ShapeDtypeStruct((n, wide), F32),
+            jax.ShapeDtypeStruct((n, wide), BF16),
             grad,
             grad,
             grad,
             jax.ShapeDtypeStruct((3, ff), F32),
         ),
         in_specs=[hbm, hbm, vm, hbm, hbm, hbm],
-        out_specs=(hbm, hbm, hbm, hbm, vm),
+        out_specs=(hbm,) * 5,
         scratch_shapes=[pltpu.VMEM(shape, dtype) for shape, dtype in scratch]
         + [
-            pltpu.SemaphoreType.DMA((COPIES,)),
-            pltpu.SemaphoreType.DMA((COPIES,)),
-            pltpu.SemaphoreType.DMA((12,)),
+            pltpu.SemaphoreType.DMA((TURNS,)),
+            pltpu.SemaphoreType.DMA((ARRIVALS,)),
+            pltpu.SemaphoreType.DMA((15,)),
         ],
         compiler_params=pltpu.CompilerParams(
             collective_id=0, has_side_effects=True, vmem_limit_bytes=67043328
         ),
         name="ffn_backward",
     )(tokens, grad_out, gain, gate_weight.T, up_weight.T, down_weight.T)
-    grad_in = (grad_out.astype(F32) + total).astype(BF16)
+    found = (grad_in, grad_gate, grad_up, grad_down, squares)
+    results = pl.pallas_call(
+        deliver,
+        out_shape=tuple(jax.ShapeDtypeStruct(a.shape, a.dtype) for a in found),
+        in_specs=[hbm] * 5,
+        out_specs=(hbm,) * 5,
+        scratch_shapes=[pltpu.VMEM(a.shape, a.dtype) for a in found]
+        + [pltpu.SemaphoreType.DMA((8,)), pltpu.SemaphoreType.DMA((8,))],
+        name="deliver",
+    )(*found)
+    grad_in, grad_gate, grad_up, grad_down, squares = results
     return grad_in, grad_gate.T, grad_up.T, grad_down.T, squares
 
 

time: 107 us -> 94.7 us (0.89)
  Pallas kernels: 101 us -> 93.8 us
  local copies, waits for them, and re-layouts: 3.14 us -> 0 us
  other arithmetic: 2.3 us -> 0 us
    pallas_call x1 -> x2, Pallas kernels: 101 us -> 93.8 us  [the longest x1 91.8 us: on_device(): pl.pallas_call(kernel, out_shape=(jax.ShapeDtypeStruct((n, wide), BF16),...]
    unnamed x12 -> x0, local copies, waits for them, and re-layouts: 3.14 us -> none
    convert_element_type x1 -> x0, other arithmetic: 2.3 us -> none  [on_device(): grad_in = (grad_out.astype(F32) + total).astype(BF16)]
where the time goes in v3:
time: 94.7 us; the launch traced here: 94.6 us
  Pallas kernels  93.8 us (99%)
    pallas_call x1, Pallas kernels, on_device(): pl.pallas_call(kernel, out_shape=(jax.ShapeDtypeStruct((n, wide), BF16),...  91.8 us
    pallas_call x1, Pallas kernels, on_device(): pl.pallas_call(deliver, out_shape=tuple((jax.ShapeDtypeStruct(a.shape, a....  2 us

profile of v3, /device:TPU:32, one launch (start us, length us, event | category | flops | bytes accessed | tf_op | source)
XLA Modules:
  0.0 94.6 jit_solution(17857050765538978697)
XLA Ops:
  0.6 91.8 %ffn_backward.1 = (bf16[1024,256]{1,0:T(8,128)(2,1)}, f32[64,384]{1,0:T(8,128)}, f32[64,384]{1,0:T(8,128)}, f32[64,384]{1,0:T(8,128)}, f32[3,384]{1,0:T(4,128)}) custom-call(bf16[1024,256]{1,0:T(8,128)(2,1)} %tok.1, bf16[1024,256]{1,0:T(8,128)(2,1)} %grd.1, f32[8,1,256]{2,1,0:T(1,128)} %bitcast.10, bf16[64,384]{1,0:T(8,128)(2,1)} %bitcast.7, ...), custom_call_target="tpu_custom_call" | custom-call | tf_op jit(solution)/shard_map/ffn_backward/pallas_call | solution.py:631
  92.4 2.0 %deliver.1 = (bf16[1024,256]{1,0:T(8,128)(2,1)}, f32[64,384]{1,0:T(8,128)}, f32[64,384]{1,0:T(8,128)}, f32[64,384]{1,0:T(8,128)}, f32[3,384]{1,0:T(4,128)}) custom-call(bf16[1024,256]{1,0:T(8,128)(2,1)} %get-tuple-element.15.refs_0_, f32[64,384]{1,0:T(8,128)} %get-tuple-element.16.refs_1_, f32[64,384]{1,0:T(8,128)} %get-tuple-element.17.refs_2_, ...), custom_call_target="tpu_custom_call" | custom-call | tf_op jit(solution)/shard_map/deliver/pallas_call | solution.py:654

commit v4 on v3

--- a/solution.py
+++ b/solution.py
@@ -11,44 +11,39 @@
 NZ, NX, NY, NC = 8, 4, 4, 2
 F32, BF16 = jnp.float32, jnp.bfloat16
 CHUNKS = 4
-ARRIVALS = 139
-TURNS = 56
+ARRIVALS = 138
+KINDS = 19
 SPANS = ((0, 256), (256, 256), (512, 256), (768, 128), (896, 128))
 ORDER = (4, 3, -3, 2, -2, 1, -1, 0)
 
 
 class Net:
     def __init__(self, send_sems, recv_sems):
-        self.send_sems, self.recv_sems, self.copies = send_sems, recv_sems, []
-        self.groups, self.used = {}, 0
-
-    def send(self, src, dst, group=None, **to):
-        at = len(self.copies)
-        if at >= TURNS:
-            self.copies[at - TURNS].wait_send()
-        if group is None:
-            group = ("one", at)
-        if group not in self.groups:
+        self.send_sems, self.recv_sems = send_sems, recv_sems
+        self.kinds, self.groups, self.used = [], {}, 0
+
+    def send(self, kind, src, dst, group=None, **to):
+        if kind not in self.kinds:
+            self.kinds.append(kind)
+        if group not in self.groups or group is None:
             self.groups[group] = self.used
             self.used += 1
         copy = pltpu.make_async_remote_copy(
             src_ref=src,
             dst_ref=dst,
-            send_sem=self.send_sems.at[at % TURNS],
+            send_sem=self.send_sems.at[self.kinds.index(kind)],
             recv_sem=self.recv_sems.at[self.groups[group]],
             device_id=to,
             device_id_type=pl.DeviceIdType.MESH,
         )
         copy.start()
-        self.copies.append(copy)
         return copy
 
     def arrived(self, group, size):
         pltpu.make_async_copy(size, size, self.recv_sems.at[self.groups[group]]).wait()
 
-    def finish(self):
-        for copy in self.copies[-TURNS:]:
-            copy.wait_send()
+    def sent(self, kind, size):
+        pltpu.make_async_copy(size, size, self.send_sems.at[self.kinds.index(kind)]).wait()
 
 
 def lanes_summed(v):
@@ -67,7 +62,7 @@
     out_in, out_g, out_u, out_d, out_sq,
     T, G, N, GU, DN, AB, H, INV, V, DGU, DDN,
     SX1, RX1, SX2, RX2, XR, SZ, RZ, SD, RD, FD, SE1, RE1, SE2, RE2,
-    PP, PR, S1, R1, S2, R2, QX, QZ, IN, LG, LU, LD, SQ,
+    PP, PR, S1, R1, S2, R2, QA, IN, LG, LU, LD, SQ,
     send_sems, recv_sems, local_sems,
 ):
     z, x, y, c = (lax.axis_index(a) for a in ("z", "x", "y", "c"))
@@ -114,16 +109,16 @@
     gz, gx, dx, dz, ya, yb = {}, {}, {}, {}, {}, {}
 
     def gx_send(d, src):
-        gx[d, 1] = net.send(src, GU.at[zz(d), x], x=xx(1))
-        gx[d, -1] = net.send(src, GU.at[zz(d), x], x=xx(-1))
+        gx[d, 1] = net.send("gx", src, GU.at[zz(d), x], x=xx(1))
+        gx[d, -1] = net.send("gx", src, GU.at[zz(d), x], x=xx(-1))
 
     def gx_pass(d):
         gx[d, 1].wait_recv()
         ref = GU.at[zz(d), xx(-1), :, gate]
-        net.send(ref, ref, "gxf", x=xx(1))
+        net.send("gxf", ref, ref, "gxf", x=xx(1))
         gx[d, -1].wait_recv()
         ref = GU.at[zz(d), xx(1), :, up]
-        net.send(ref, ref, "gxf", x=xx(-1))
+        net.send("gxf", ref, ref, "gxf", x=xx(-1))
 
     def gz_step(s):
         for way in (1, -1):
@@ -132,7 +127,7 @@
                 ref = GU.at[zz(-way * s), x]
                 if s == NZ // 2 - 1:
                     ref = GU.at[zz(-way * s), x, :, gate if way == 1 else up]
-                gz[s + 1, way] = net.send(ref, ref, z=zz(way))
+                gz[s + 1, way] = net.send("gz", ref, ref, z=zz(way))
         if s < NZ // 2:
             gx_send(-s, GU.at[zz(-s), x])
             gx_send(s, GU.at[zz(s), x])
@@ -142,10 +137,10 @@
     def dx_pass():
         dx[1].wait_recv()
         ref = DN.at[z, xx(-1), pl.ds(0, half_part)]
-        net.send(ref, ref, "dxf", x=xx(1))
+        net.send("dxf", ref, ref, "dxf", x=xx(1))
         dx[-1].wait_recv()
         ref = DN.at[z, xx(1), pl.ds(half_part, half_part)]
-        net.send(ref, ref, "dxf", x=xx(-1))
+        net.send("dxf", ref, ref, "dxf", x=xx(-1))
 
     def dz_step(s, *pieces):
         for dx_ in pieces:
@@ -154,27 +149,27 @@
                     dz[s, dx_, way].wait_recv()
                 ref = DN.at[zz(-way * s), xx(dx_)]
                 if s < NZ // 2 - 1:
-                    dz[s + 1, dx_, way] = net.send(ref, ref, z=zz(way))
+                    dz[s + 1, dx_, way] = net.send("dz", ref, ref, z=zz(way))
                 elif (dx_ in (0, -1)) == (way == 1):
-                    net.send(ref, ref, "dz", z=zz(way))
+                    net.send("dz", ref, ref, "dz", z=zz(way))
 
     def y_own(ch):
         for way in (1, -1):
-            ya["T", ch, way] = net.send(T.at[me, some(ch)], T.at[me, some(ch)], y=yy(way))
-            ya["G", ch, way] = net.send(G.at[me, some(ch)], G.at[me, some(ch)], y=yy(way))
+            ya["T", ch, way] = net.send("ya", T.at[me, some(ch)], T.at[me, some(ch)], y=yy(way))
+            ya["G", ch, way] = net.send("ya", G.at[me, some(ch)], G.at[me, some(ch)], y=yy(way))
 
     def to_other(name, full, d, ch):
         ref = full.at[slot(d), some(ch)]
-        net.send(ref, ref, ("c", ch), c=other)
+        net.send("c", ref, ref, ("c", ch), c=other)
 
     def y_pass(ch):
         ya["T", ch, 1].wait_recv()
         ref = T.at[slot(-1), some(ch)]
-        yb["T", ch] = net.send(ref, ref, y=yy(1))
+        yb["T", ch] = net.send("yb", ref, ref, y=yy(1))
         to_other("T", T, -1, ch)
         ya["G", ch, -1].wait_recv()
         ref = G.at[slot(1), some(ch)]
-        yb["G", ch] = net.send(ref, ref, y=yy(-1))
+        yb["G", ch] = net.send("yb", ref, ref, y=yy(-1))
         to_other("G", G, 1, ch)
         ya["G", ch, 1].wait_recv()
         to_other("G", G, -1, ch)
@@ -251,18 +246,18 @@
         k = zz(ORDER[i])
         SX1[i, 0] = DGU[k, xx(2), :, gate].astype(BF16)
         SX1[i, 1] = DGU[k, xx(2), :, up].astype(BF16)
-        net.send(SX1.at[i, 0], RX1.at[i, 0], ("x1", i), x=xx(1))
-        net.send(SX1.at[i, 1], RX1.at[i, 1], ("x1", i), x=xx(-1))
+        net.send("x1", SX1.at[i, 0], RX1.at[i, 0], ("x1", i), x=xx(1))
+        net.send("x1", SX1.at[i, 1], RX1.at[i, 1], ("x1", i), x=xx(-1))
 
     def x_step2(i):
         k = zz(ORDER[i])
         net.arrived(("x1", i), SX1.at[i])
         SX2[i, 0, :, gate] = (DGU[k, xx(1), :, gate] + RX1[i, 0].astype(F32)).astype(BF16)
         SX2[i, 0, :, up] = DGU[k, xx(1), :, up].astype(BF16)
-        net.send(SX2.at[i, 0], RX2.at[i, 0], ("x2", i), x=xx(1))
+        net.send("x2", SX2.at[i, 0], RX2.at[i, 0], ("x2", i), x=xx(1))
         SX2[i, 1, :, gate] = DGU[k, xx(-1), :, gate].astype(BF16)
         SX2[i, 1, :, up] = (DGU[k, xx(-1), :, up] + RX1[i, 1].astype(F32)).astype(BF16)
-        net.send(SX2.at[i, 1], RX2.at[i, 1], ("x2", i), x=xx(-1))
+        net.send("x2", SX2.at[i, 1], RX2.at[i, 1], ("x2", i), x=xx(-1))
 
     def x_sum(i):
         net.arrived(("x2", i), SX2.at[i])
@@ -273,8 +268,8 @@
         value = x_sum(i)
         if d == NZ // 2:
             SZ[0, 0] = value.astype(BF16)
-            zs[1, d] = net.send(SZ.at[0, 0, :, gate], RZ.at[0, 0, :, gate], z=zz(1))
-            zs[-1, d] = net.send(SZ.at[0, 0, :, up], RZ.at[0, 1, :, up], z=zz(-1))
+            zs[1, d] = net.send("zs", SZ.at[0, 0, :, gate], RZ.at[0, 0, :, gate], z=zz(1))
+            zs[-1, d] = net.send("zs", SZ.at[0, 0, :, up], RZ.at[0, 1, :, up], z=zz(-1))
             return None
         ways = (1, -1) if d == 0 else (1 if d > 0 else -1,)
         for way in ways:
@@ -289,7 +284,7 @@
                 value = value + RZ[s - 1, w].astype(F32)
             if d != 0:
                 SZ[s, w] = value.astype(BF16)
-                zs[way, abs(d)] = net.send(SZ.at[s, w], RZ.at[s, w], z=zz(way))
+                zs[way, abs(d)] = net.send("zs", SZ.at[s, w], RZ.at[s, w], z=zz(way))
         return value
 
     def d_step(d, way, half):
@@ -303,7 +298,7 @@
             value = value + RD[s - 1, w, blocks].astype(F32)
         SD[s, w, blocks] = value.astype(BF16)
         group = "ds" if abs(d) == 1 else None
-        ds[way, half, abs(d)] = net.send(
+        ds[way, half, abs(d)] = net.send("ds",
             SD.at[s, w, blocks], RD.at[s, w, blocks], group, z=zz(way)
         )
 
@@ -319,25 +314,25 @@
     def e_step1():
         SE1[...] = FD[xx(2)].astype(BF16)
         lo, hi = pl.ds(0, half_part), pl.ds(half_part, half_part)
-        net.send(SE1.at[lo], RE1.at[lo], "e1", x=xx(1))
-        net.send(SE1.at[hi], RE1.at[hi], "e1", x=xx(-1))
+        net.send("e1", SE1.at[lo], RE1.at[lo], "e1", x=xx(1))
+        net.send("e1", SE1.at[hi], RE1.at[hi], "e1", x=xx(-1))
 
     def e_step2():
         lo, hi = pl.ds(0, half_part), pl.ds(half_part, half_part)
         net.arrived("e1", SE1)
         SE2[0, lo] = (FD[xx(1), lo] + RE1[lo].astype(F32)).astype(BF16)
         SE2[0, hi] = FD[xx(1), hi].astype(BF16)
-        net.send(SE2.at[0], RE2.at[0], "e2", x=xx(1))
+        net.send("e2", SE2.at[0], RE2.at[0], "e2", x=xx(1))
         SE2[1, lo] = FD[xx(-1), lo].astype(BF16)
         SE2[1, hi] = (FD[xx(-1), hi] + RE1[hi].astype(F32)).astype(BF16)
-        net.send(SE2.at[1], RE2.at[1], "e2", x=xx(-1))
+        net.send("e2", SE2.at[1], RE2.at[1], "e2", x=xx(-1))
 
     def e_sum():
         net.arrived("e2", SE2)
         return FD[x] + RE2[0].astype(F32) + RE2[1].astype(F32)
 
     def p_send(ch):
-        pc[ch] = net.send(PP.at[other, :, span(ch)], PR.at[:, span(ch)], c=other)
+        pc[ch] = net.send("pc", PP.at[other, :, span(ch)], PR.at[:, span(ch)], c=other)
 
     def p_pair(ch, d, at, n):
         sub = pl.ds(ch * rows + at, n)
@@ -347,20 +342,20 @@
         pc[ch].wait_recv()
         S1[ch] = p_pair(ch, 2, 0, rows).astype(BF16)
         lo, hi = pl.ds(0, half_rows), pl.ds(half_rows, half_rows)
-        net.send(S1.at[ch, lo], R1.at[ch, lo], ("p1", ch), y=yy(1))
-        net.send(S1.at[ch, hi], R1.at[ch, hi], ("p1", ch), y=yy(-1))
+        net.send("p1", S1.at[ch, lo], R1.at[ch, lo], ("p1", ch), y=yy(1))
+        net.send("p1", S1.at[ch, hi], R1.at[ch, hi], ("p1", ch), y=yy(-1))
 
     def p_step2(ch):
         lo, hi = pl.ds(0, half_rows), pl.ds(half_rows, half_rows)
         net.arrived(("p1", ch), S1.at[ch])
         S2[ch, 0, lo] = (p_pair(ch, 1, 0, half_rows) + R1[ch, lo].astype(F32)).astype(BF16)
         S2[ch, 0, hi] = p_pair(ch, 1, half_rows, half_rows).astype(BF16)
-        net.send(S2.at[ch, 0], R2.at[ch, 0], ("p2", ch), y=yy(1))
+        net.send("p2", S2.at[ch, 0], R2.at[ch, 0], ("p2", ch), y=yy(1))
         S2[ch, 1, lo] = p_pair(ch, -1, 0, half_rows).astype(BF16)
         S2[ch, 1, hi] = (
             p_pair(ch, -1, half_rows, half_rows) + R1[ch, hi].astype(F32)
         ).astype(BF16)
-        net.send(S2.at[ch, 1], R2.at[ch, 1], ("p2", ch), y=yy(-1))
+        net.send("p2", S2.at[ch, 1], R2.at[ch, 1], ("p2", ch), y=yy(-1))
 
     stores = []
 
@@ -382,21 +377,21 @@
         for copy in locals_[2:5]:
             copy.wait()
         for way in (1, -1):
-            gz[1, way] = net.send(GU.at[z, x], GU.at[z, x], z=zz(way))
-            dx[way] = net.send(DN.at[z, x], DN.at[z, x], x=xx(way))
+            gz[1, way] = net.send("gz", GU.at[z, x], GU.at[z, x], z=zz(way))
+            dx[way] = net.send("dx", DN.at[z, x], DN.at[z, x], x=xx(way))
         dz_step(0, 0)
         gx_send(0, GU.at[z, x])
         for copy in locals_[5:]:
             copy.wait()
         y_own(1)
-        net.send(T.at[me], T.at[me], ("c", 0), c=other)
-        net.send(G.at[me], G.at[me], ("c", 0), c=other)
+        net.send("c", T.at[me], T.at[me], ("c", 0), c=other)
+        net.send("c", G.at[me], G.at[me], ("c", 0), c=other)
 
     def e_finish():
         down = e_sum()
         LD[...] = down
         store(LD, out_d)
-        QX[x, :, pl.ds(2 * ff, ff)] = jnp.sum(down * down, axis=0, keepdims=True)
+        QA[z * NX + x, :, pl.ds(2 * ff, ff)] = jnp.sum(down * down, axis=0, keepdims=True)
 
     def z_finish():
         both = z_step(steps - 1)
@@ -404,34 +399,53 @@
         LU[...] = both[:, ff : 2 * ff]
         store(LG, out_g)
         store(LU, out_u)
-        QX[x, :, pl.ds(0, 2 * ff)] = jnp.sum(both * both, axis=0, keepdims=True)
-
-    def q_x():
-        for d in (2, 1, 3):
-            net.send(QX.at[x], QX.at[x], "qx", x=xx(d))
-        p_sum(2)
-        net.arrived("qx", QX.at[pl.ds(0, NX - 1)])
-        total = QX[0]
-        for at in range(1, NX):
-            total = total + QX[at]
-        QZ[z] = total
-
-    def q_z():
-        for d in (4, 3, 5, 2, 6, 1, 7):
-            net.send(QZ.at[z], QZ.at[z], "qz", z=zz(d))
-        p_sum(3)
-        net.arrived("qz", QZ.at[pl.ds(0, NZ - 1)])
-        total = QZ[0]
-        for at in range(1, NZ):
-            total = total + QZ[at]
+        QA[z * NX + x, :, pl.ds(0, 2 * ff)] = jnp.sum(both * both, axis=0, keepdims=True)
+
+    def q_all():
+        for dz_ in (4, 3, 5, 2, 6, 1, 7, 0):
+            for dx_ in (2, 1, 3, 0):
+                if dz_ or dx_:
+                    to = {}
+                    if dz_:
+                        to["z"] = zz(dz_)
+                    if dx_:
+                        to["x"] = xx(dx_)
+                    net.send("q", QA.at[z * NX + x], QA.at[z * NX + x], "q", **to)
+        for ch in range(CHUNKS):
+            p_sum(ch)
+        net.arrived("q", QA.at[pl.ds(0, NZ * NX - 1)])
+        total = QA[0]
+        for at in range(1, NZ * NX):
+            total = total + QA[at]
         total = total / model
         for at in range(3):
             SQ[pl.ds(at, 1)] = total[:, at * ff : (at + 1) * ff]
         store(SQ, out_sq)
 
     def finish():
-        assert net.used == ARRIVALS, net.used
-        net.finish()
+        assert net.used == ARRIVALS and len(net.kinds) == KINDS, net.used
+        for kind, size in (
+            ("gz", GU.at[pl.ds(0, NZ - 1), 0]),
+            ("gx", GU.at[pl.ds(0, NZ // 2)]),
+            ("gxf", DN.at[pl.ds(0, NZ // 2)]),
+            ("dx", DN.at[0, pl.ds(0, 2)]),
+            ("dxf", DN.at[0, 0]),
+            ("dz", DN.at[pl.ds(0, NZ - 1)]),
+            ("ya", PR),
+            ("yb", PR.at[pl.ds(0, 2)]),
+            ("c", PP),
+            ("x1", SX1),
+            ("x2", SX2),
+            ("zs", SX2.at[pl.ds(0, NZ - 1), 0]),
+            ("ds", DN.at[pl.ds(0, NZ - 1)]),
+            ("e1", SE1),
+            ("e2", SE2),
+            ("pc", PR),
+            ("p1", S1),
+            ("p2", S2),
+            ("q", QA.at[pl.ds(0, NZ * NX - 1)]),
+        ):
+            net.sent(kind, size)
         for copy in stores:
             copy.wait()
 
@@ -473,11 +487,11 @@
     norm(0)
     gx_pass(4)
     y_pass(3)
+    y_ready(1)
+    norm(1)
     net.arrived("dz", DN.at[0])
     net.arrived("gxf", DN.at[pl.ds(0, 4)])
     forward(0)
-    y_ready(1)
-    norm(1)
     y_pass(4)
     forward(1)
     y_last(2)
@@ -493,64 +507,64 @@
     norm(4)
     forward(4)
 
-    ahead = 3
+    ahead = 4
     weights(ORDER[0])
     x_step1(0)
+    weights(ORDER[1])
+    x_step1(1)
     downs(ORDER[0])
     d_both(0, True)
-    weights(ORDER[1])
-    x_step1(1)
+    weights(ORDER[2])
+    x_step1(2)
     downs(ORDER[1])
     downs(ORDER[2])
     d_both(1, False)
-    weights(ORDER[2])
-    x_step1(2)
+    weights(ORDER[3])
+    x_step1(3)
     for i in range(5):
         x_step2(i)
-        weights(ORDER[i + ahead])
-        x_step1(i + ahead)
+        if i == 2:
+            d_both(2, True)
+        if i + ahead < steps:
+            weights(ORDER[i + ahead])
+            x_step1(i + ahead)
         if i == 0:
             downs(ORDER[3])
             downs(ORDER[4])
             d_both(1, True)
         if i == 1:
             d_both(2, False)
-        if i == 2:
             downs(ORDER[5])
             downs(ORDER[6])
-            d_both(2, True)
         if i == 3:
-            d_both(3, False)
-        if i == 4:
-            downs(ORDER[7])
             d_both(3, True)
         if i >= 2:
             p_step1(i - 2)
         if i < CHUNKS:
             partial(i)
             p_send(i)
+        if i == 2:
+            d_both(3, False)
+            downs(ORDER[7])
         if i >= 1:
             z_step(i - 1)
     x_step2(5)
     p_step1(3)
     p_step2(0)
     x_step2(6)
-    z_step(4)
-    x_step2(7)
     p_step2(1)
     d_sum()
     e_step1()
+    x_step2(7)
+    z_step(4)
+    p_step2(2)
     z_step(5)
-    p_step2(2)
+    p_step2(3)
     z_step(6)
     e_step2()
-    p_step2(3)
-    p_sum(0)
-    p_sum(1)
     z_finish()
     e_finish()
-    q_x()
-    q_z()
+    q_all()
     finish()
 
 
@@ -619,8 +633,7 @@
         ((CHUNKS, rows, wide), BF16),
         ((CHUNKS, 2, rows, wide), BF16),
         ((CHUNKS, 2, rows, wide), BF16),
-        ((NX, 1, 3 * ff), F32),
-        ((NZ, 1, 3 * ff), F32),
+        ((NZ * NX, 1, 3 * ff), F32),
         ((n, wide), BF16),
         ((part, ff), F32),
         ((part, ff), F32),
@@ -641,7 +654,7 @@
         out_specs=(hbm,) * 5,
         scratch_shapes=[pltpu.VMEM(shape, dtype) for shape, dtype in scratch]
         + [
-            pltpu.SemaphoreType.DMA((TURNS,)),
+            pltpu.SemaphoreType.DMA((KINDS,)),
             pltpu.SemaphoreType.DMA((ARRIVALS,)),
             pltpu.SemaphoreType.DMA((15,)),
         ],

time: 94.7 us -> 93.5 us (0.987)
  Pallas kernels: 93.8 us -> 92.5 us
    pallas_call x1, Pallas kernels: 91.8 us -> 90.5 us  [on_device(): pl.pallas_call(kernel, out_shape=(jax.ShapeDtypeStruct((n, wide), BF16),...]
where the time goes in v4:
time: 93.5 us; the launch traced here: 93.3 us
  Pallas kernels  92.5 us (99%)
    pallas_call x1, Pallas kernels, on_device(): pl.pallas_call(kernel, out_shape=(jax.ShapeDtypeStruct((n, wide), BF16),...  90.5 us
    pallas_call x1, Pallas kernels, on_device(): pl.pallas_call(deliver, out_shape=tuple((jax.ShapeDtypeStruct(a.shape, a....  2 us

profile of v4, /device:TPU:32, one launch (start us, length us, event | category | flops | bytes accessed | tf_op | source)
XLA Modules:
  0.0 93.3 jit_solution(8015662095369514463)
XLA Ops:
  0.6 90.5 %ffn_backward.1 = (bf16[1024,256]{1,0:T(8,128)(2,1)}, f32[64,384]{1,0:T(8,128)}, f32[64,384]{1,0:T(8,128)}, f32[64,384]{1,0:T(8,128)}, f32[3,384]{1,0:T(4,128)}) custom-call(bf16[1024,256]{1,0:T(8,128)(2,1)} %tok.1, bf16[1024,256]{1,0:T(8,128)(2,1)} %grd.1, f32[8,1,256]{2,1,0:T(1,128)} %bitcast.10, bf16[64,384]{1,0:T(8,128)(2,1)} %bitcast.7, ...), custom_call_target="tpu_custom_call" | custom-call | tf_op jit(solution)/shard_map/ffn_backward/pallas_call | solution.py:644
  91.2 2.0 %deliver.1 = (bf16[1024,256]{1,0:T(8,128)(2,1)}, f32[64,384]{1,0:T(8,128)}, f32[64,384]{1,0:T(8,128)}, f32[64,384]{1,0:T(8,128)}, f32[3,384]{1,0:T(4,128)}) custom-call(bf16[1024,256]{1,0:T(8,128)(2,1)} %get-tuple-element.15.refs_0_, f32[64,384]{1,0:T(8,128)} %get-tuple-element.16.refs_1_, f32[64,384]{1,0:T(8,128)} %get-tuple-element.17.refs_2_, ...), custom_call_target="tpu_custom_call" | custom-call | tf_op jit(solution)/shard_map/deliver/pallas_call | solution.py:667

commit v5 on v4

--- a/solution.py
+++ b/solution.py
@@ -58,11 +58,11 @@
 
 
 def kernel(
-    tok, grd, gain, wg, wu, wd,
+    tok, grd, gains, wg, wu, wd,
     out_in, out_g, out_u, out_d, out_sq,
     T, G, N, GU, DN, AB, H, INV, V, DGU, DDN,
     SX1, RX1, SX2, RX2, XR, SZ, RZ, SD, RD, FD, SE1, RE1, SE2, RE2,
-    PP, PR, S1, R1, S2, R2, QA, IN, LG, LU, LD, SQ,
+    PP, PR, S1, R1, S2, R2, QA, IN, LG, LU, LD, SQ, gain,
     send_sems, recv_sems, local_sems,
 ):
     z, x, y, c = (lax.axis_index(a) for a in ("z", "x", "y", "c"))
@@ -97,6 +97,7 @@
         (wu, GU.at[z, x, :, up]),
         (tok.at[rest], T.at[me, rest]),
         (grd.at[rest], G.at[me, rest]),
+        (gains, gain),
     )
     locals_ = [
         pltpu.make_async_copy(src, dst, local_sems.at[i]) for i, (src, dst) in enumerate(loads)
@@ -516,11 +517,11 @@
     d_both(0, True)
     weights(ORDER[2])
     x_step1(2)
+    weights(ORDER[3])
+    x_step1(3)
     downs(ORDER[1])
     downs(ORDER[2])
     d_both(1, False)
-    weights(ORDER[3])
-    x_step1(3)
     for i in range(5):
         x_step2(i)
         if i == 2:
@@ -598,7 +599,6 @@
     blocks = NY * NC
     rows = n // CHUNKS
     gain = norm_gain.reshape(blocks, 1, wide)
-    vm = pl.BlockSpec(memory_space=pltpu.VMEM)
     hbm = pl.BlockSpec(memory_space=pl.ANY)
     half = NZ // 2
     scratch = [
@@ -639,6 +639,7 @@
         ((part, ff), F32),
         ((part, ff), F32),
         ((3, ff), F32),
+        ((blocks, 1, wide), F32),
     ]
     grad = jax.ShapeDtypeStruct((part, ff), F32)
     grad_in, grad_gate, grad_up, grad_down, squares = pl.pallas_call(
@@ -650,13 +651,13 @@
             grad,
             jax.ShapeDtypeStruct((3, ff), F32),
         ),
-        in_specs=[hbm, hbm, vm, hbm, hbm, hbm],
+        in_specs=[hbm] * 6,
         out_specs=(hbm,) * 5,
         scratch_shapes=[pltpu.VMEM(shape, dtype) for shape, dtype in scratch]
         + [
             pltpu.SemaphoreType.DMA((KINDS,)),
             pltpu.SemaphoreType.DMA((ARRIVALS,)),
-            pltpu.SemaphoreType.DMA((15,)),
+            pltpu.SemaphoreType.DMA((16,)),
         ],
         compiler_params=pltpu.CompilerParams(
             collective_id=0, has_side_effects=True, vmem_limit_bytes=67043328

time: 93.5 us -> 91.9 us (0.983)
  Pallas kernels: 92.5 us -> 91 us
    pallas_call x1, Pallas kernels: 90.5 us -> 89 us  [on_device(): pl.pallas_call(kernel, out_shape=(jax.ShapeDtypeStruct((n, wide), BF16),...]
where the time goes in v5:
time: 91.9 us; the launch traced here: 91.8 us
  Pallas kernels  91 us (99%)
    pallas_call x1, Pallas kernels, on_device(): pl.pallas_call(kernel, out_shape=(jax.ShapeDtypeStruct((n, wide), BF16),...  89 us
    pallas_call x1, Pallas kernels, on_device(): pl.pallas_call(deliver, out_shape=tuple((jax.ShapeDtypeStruct(a.shape, a....  2 us

profile of v5, /device:TPU:32, one launch (start us, length us, event | category | flops | bytes accessed | tf_op | source)
XLA Modules:
  0.0 91.8 jit_solution(6880241529281373618)
XLA Ops:
  0.6 89.0 %ffn_backward.1 = (bf16[1024,256]{1,0:T(8,128)(2,1)}, f32[64,384]{1,0:T(8,128)}, f32[64,384]{1,0:T(8,128)}, f32[64,384]{1,0:T(8,128)}, f32[3,384]{1,0:T(4,128)}) custom-call(bf16[1024,256]{1,0:T(8,128)(2,1)} %tok.1, bf16[1024,256]{1,0:T(8,128)(2,1)} %grd.1, f32[8,1,256]{2,1,0:T(1,128)} %bitcast.10, bf16[64,384]{1,0:T(8,128)(2,1)} %bitcast.7, ...), custom_call_target="tpu_custom_call" | custom-call | tf_op jit(solution)/shard_map/ffn_backward/pallas_call | solution.py:645
  89.6 2.0 %deliver.1 = (bf16[1024,256]{1,0:T(8,128)(2,1)}, f32[64,384]{1,0:T(8,128)}, f32[64,384]{1,0:T(8,128)}, f32[64,384]{1,0:T(8,128)}, f32[3,384]{1,0:T(4,128)}) custom-call(bf16[1024,256]{1,0:T(8,128)(2,1)} %get-tuple-element.15.refs_0_, f32[64,384]{1,0:T(8,128)} %get-tuple-element.16.refs_1_, f32[64,384]{1,0:T(8,128)} %get-tuple-element.17.refs_2_, ...), custom_call_target="tpu_custom_call" | custom-call | tf_op jit(solution)/shard_map/deliver/pallas_call | solution.py:668

commit v6 on v5

--- a/solution.py
+++ b/solution.py
@@ -554,9 +554,9 @@
     p_step2(0)
     x_step2(6)
     p_step2(1)
+    x_step2(7)
     d_sum()
     e_step1()
-    x_step2(7)
     z_step(4)
     p_step2(2)
     z_step(5)

time: 91.9 us -> 91.6 us (level)
  no operation moved by 1% of the time
where the time goes in v6:
time: 91.6 us; the launch traced here: 91.4 us
  Pallas kernels  90.6 us (99%)
    pallas_call x1, Pallas kernels, on_device(): pl.pallas_call(kernel, out_shape=(jax.ShapeDtypeStruct((n, wide), BF16),...  88.6 us
    pallas_call x1, Pallas kernels, on_device(): pl.pallas_call(deliver, out_shape=tuple((jax.ShapeDtypeStruct(a.shape, a....  2 us

profile of v6, /device:TPU:32, one launch (start us, length us, event | category | flops | bytes accessed | tf_op | source)
XLA Modules:
  0.0 91.4 jit_solution(9117131654043814725)
XLA Ops:
  0.6 88.6 %ffn_backward.1 = (bf16[1024,256]{1,0:T(8,128)(2,1)}, f32[64,384]{1,0:T(8,128)}, f32[64,384]{1,0:T(8,128)}, f32[64,384]{1,0:T(8,128)}, f32[3,384]{1,0:T(4,128)}) custom-call(bf16[1024,256]{1,0:T(8,128)(2,1)} %tok.1, bf16[1024,256]{1,0:T(8,128)(2,1)} %grd.1, f32[8,1,256]{2,1,0:T(1,128)} %bitcast.10, bf16[64,384]{1,0:T(8,128)(2,1)} %bitcast.7, ...), custom_call_target="tpu_custom_call" | custom-call | tf_op jit(solution)/shard_map/ffn_backward/pallas_call | solution.py:645
  89.2 2.0 %deliver.1 = (bf16[1024,256]{1,0:T(8,128)(2,1)}, f32[64,384]{1,0:T(8,128)}, f32[64,384]{1,0:T(8,128)}, f32[64,384]{1,0:T(8,128)}, f32[3,384]{1,0:T(4,128)}) custom-call(bf16[1024,256]{1,0:T(8,128)(2,1)} %get-tuple-element.15.refs_0_, f32[64,384]{1,0:T(8,128)} %get-tuple-element.16.refs_1_, f32[64,384]{1,0:T(8,128)} %get-tuple-element.17.refs_2_, ...), custom_call_target="tpu_custom_call" | custom-call | tf_op jit(solution)/shard_map/deliver/pallas_call | solution.py:668
